TPU v7x, 128 devices: a whole 4x4x4 slice. The times are simulated.
128 devices in a mesh: ep: 16 (over z, x), tp: 8 (over y, core).
Axes of the slice: x: 4, y: 4, z: 4, core: 2. Of those that a mesh axis runs over, the one named last changes fastest.
Arguments:
- mixer_rows: bfloat16 [4096, 4096], P('ep'), may hold values from -8 to 8, as said below
- mixer_gain: float32 [4096], replicated, may hold values from 0.1 to 1.9
- gate_proj: bfloat16 [4096, 4096], P(None, 'tp'), may hold values from -0.09375 to 0.09375
- input_proj: bfloat16 [4096, 4096], P(None, 'tp'), may hold values from -0.09375 to 0.09375
- conv_taps: float32 [4, 4096], P(None, 'tp'), may hold values from -2 to 2
- input_gates: bfloat16 [16, 256, 256], P('tp'), may hold values from -0.375 to 0.375
- decay_gates: bfloat16 [16, 256, 256], P('tp'), may hold values from -0.375 to 0.375
- decay_offset: float32 [4096], P('tp'), may hold values from 4.8 to 13, as said below
- out_proj: bfloat16 [4096, 4096], P('tp'), may hold values from -0.09375 to 0.09375
- mixer_scale: float32 [4096], replicated, may hold values from 0.1 to 1.9
- expert_rows: bfloat16 [4096, 4096], P('ep'), may hold values from -6 to 6
- expert_gain: float32 [4096], replicated, may hold values from 0.1 to 1.9
- route_ids: int32 [4096, 2], P('ep'), may hold values from 0 to 15, all different within a row; in each aligned block of 256 rows (0 to 255, 256 to 511, ...) at most 48 rows name the same one
- route_weights: float32 [4096, 2], P('ep'), may hold values from 0.5 to 2
- expert_gate: bfloat16 [16, 4096, 1024], P('ep', None, 'tp'), may hold values from -0.09375 to 0.09375
- expert_up: bfloat16 [16, 4096, 1024], P('ep', None, 'tp'), may hold values from -0.09375 to 0.09375
- expert_down: bfloat16 [16, 1024, 4096], P('ep', 'tp'), may hold values from -0.1875 to 0.1875
- shared_gate: bfloat16 [4096, 1024], P(None, 'tp'), may hold values from -0.09375 to 0.09375
- shared_up: bfloat16 [4096, 1024], P(None, 'tp'), may hold values from -0.09375 to 0.09375
- shared_down: bfloat16 [1024, 4096], P('tp'), may hold values from -0.1875 to 0.1875
- expert_scale: float32 [4096], replicated, may hold values from 0.1 to 1.9
Outputs:
- mixer_out: bfloat16 [4096, 4096], P(('ep', 'tp'))
- expert_out: bfloat16 [4096, 4096], P(('ep', 'tp'))
Inputs may be any that keep to these rules, and one draw needn't show every extreme that they name: `mixer_rows`: order one, with a common direction whose weight drifts slowly along the sequence. `decay_offset`: the even channels forget within some 30 to 200 tokens; the odd channels keep 5 to 90 percent of their state over the whole sequence of 4096 tokens. `route_ids`: each row names 2 different experts; within the rows of one index of ep (aligned blocks of 256 rows) no expert is named by more than 48 rows, and in some blocks one is named by exactly 48.
All inputs are finite; a program needn't handle non-finite values.
Results may differ from a plain program's by a relative error of at most 0.0033.
The roundings to bfloat16 on the way count: a program that leaves them out, or rounds other values in their place, can miss the bound.
Values may be sent and summed in bfloat16 or wider, within the bound.
No kernel may reach another device: no remote copies, remote signals or barrier semaphores. Data moves between devices by JAX's collectives and lax.ppermute only.
A program may use at most 192 MiB of HBM per device.

v0:
```python
import jax
import jax.numpy as jnp
from jax import lax
from jax.sharding import PartitionSpec as P

eps = 1e-06
lru_power = 8.0


def shifted(block, axis, distance):
    devices = range(lax.axis_size(axis))
    route = [(i - distance, i) for i in devices if i - distance in devices]
    return lax.ppermute(block, axis, route)


def sent_to_all(shard, axis):
    length = lax.axis_size(axis)
    return lax.all_to_all(
        jnp.broadcast_to(shard[None], (length, *shard.shape)), axis, 0, 0, tiled=True
    )


def collected_together(shard, axis):
    leaves = jax.tree.leaves(shard)
    turns = sorted(range(len(leaves)), key=lambda k: -leaves[k].size)
    width = (1, *leaves[turns[0]].shape)[-1]
    lines = [
        jnp.pad(leaves[k].reshape(-1), (0, -leaves[k].size % width)).reshape(-1, width)
        for k in turns
    ]
    both, at, found = (sent_to_all(jnp.concatenate(lines), axis), 0, {})
    for k, line in zip(turns, lines):
        share = both[:, at : at + len(line)].reshape(len(both), -1)
        found[k] = share[:, : leaves[k].size].reshape(-1, *leaves[k].shape)
        at += len(line)
    numbers = iter(range(len(leaves)))
    return jax.tree.map(lambda _: found[next(numbers)], shard)


def folded_in_pairs(pieces, combine):
    while len(jax.tree.leaves(pieces)[0]) > 1:
        pieces = jax.vmap(combine)(
            *(jax.tree.map(lambda part: part[side::2], pieces) for side in (0, 1))
        )
    return jax.tree.map(lambda part: part[0], pieces)


def carried_in(shard, axis, combine, identity):
    length, mine = (lax.axis_size(axis), lax.axis_index(axis))
    passed = jnp.arange(length) < mine

    def kept(part, zero, own):
        part = jnp.where(
            passed.reshape(-1, *(1 for _ in own.shape)), part, jnp.asarray(zero, own.dtype)
        )
        return part

    pieces = collected_together(shard, axis)
    return folded_in_pairs(jax.tree.map(kept, pieces, identity, shard), combine)


def sent_together(arrays, axis, dim, along):
    both = jnp.concatenate(arrays, axis=along)
    whole, at, outs = (lax.psum_scatter(both, axis, scatter_dimension=dim, tiled=True), 0, [])
    for a in arrays:
        outs.append(lax.slice_in_dim(whole, at, at + a.shape[along], axis=along))
        at += a.shape[along]
    return tuple(outs)


def rms_scale(values, scale):
    floats = values.astype(jnp.float32)
    return floats * lax.rsqrt(jnp.mean(floats * floats, axis=-1, keepdims=True) + eps) * scale


def linear_pair(earlier, later):
    return (earlier[0] * later[0], later[0] * earlier[1] + later[1])


def slot_table(route_ids, expert_count, capacity):
    id_list = route_ids.reshape(-1)
    indicator = (id_list[:, None] == jnp.arange(expert_count, dtype=jnp.int32)[None, :]).astype(
        jnp.int32
    )
    earlier_count = jnp.cumsum(indicator, axis=0) - indicator
    position = jnp.sum(earlier_count * indicator, axis=1)
    slot_ids = id_list * capacity + position
    matched = (
        slot_ids[None, :] == jnp.arange(expert_count * capacity, dtype=jnp.int32)[:, None]
    ).astype(jnp.int32)
    source = jnp.sum(matched * jnp.arange(id_list.shape[0], dtype=jnp.int32)[None, :], axis=1)
    filled = jnp.sum(matched, axis=1) > 0
    return (slot_ids, source, filled)


def body(
    mixer_rows,
    mixer_gain,
    gate_proj,
    input_proj,
    conv_taps,
    input_gates,
    decay_gates,
    decay_offset,
    out_proj,
    mixer_scale,
    expert_rows,
    expert_gain,
    route_ids,
    route_weights,
    expert_gate,
    expert_up,
    expert_down,
    shared_gate,
    shared_up,
    shared_down,
    expert_scale,
):
    row_count = mixer_rows.shape[0]
    normed = rms_scale(mixer_rows, mixer_gain).astype(jnp.bfloat16)
    gate_branch = jax.nn.gelu(jnp.dot(normed, gate_proj, preferred_element_type=jnp.float32))
    branch = jnp.dot(normed, input_proj, preferred_element_type=jnp.float32).astype(jnp.bfloat16)
    tap_count = conv_taps.shape[0]
    earlier_rows = shifted(branch[row_count - tap_count + 1 :], "ep", 1)
    padded = jnp.concatenate([earlier_rows, branch], axis=0)
    conv_sum = conv_taps[0] * padded[0:row_count].astype(jnp.float32)
    for tap_index in range(1, tap_count):
        conv_sum = conv_sum + conv_taps[tap_index] * padded[
            tap_index : tap_index + row_count
        ].astype(jnp.float32)
    conv_out = conv_sum.astype(jnp.bfloat16)
    block_rows = conv_out.reshape(row_count, input_gates.shape[0], input_gates.shape[1])
    input_gate = jax.nn.sigmoid(
        jnp.einsum("rbi,bij->rbj", block_rows, input_gates, preferred_element_type=jnp.float32)
    ).reshape(row_count, -1)
    decay_gate = jax.nn.sigmoid(
        jnp.einsum("rbi,bij->rbj", block_rows, decay_gates, preferred_element_type=jnp.float32)
    ).reshape(row_count, -1)
    log_decay = -lru_power * decay_gate * jax.nn.softplus(-decay_offset)
    positions = lax.axis_index("ep") * row_count + jnp.arange(row_count, dtype=jnp.int32)
    input_scale = jnp.where((positions == 0)[:, None], 1.0, jnp.sqrt(-jnp.expm1(2.0 * log_decay)))
    drive_term = input_scale * input_gate * conv_out.astype(jnp.float32)
    decay_rate = jnp.exp(log_decay)
    decay_product, local_states = lax.associative_scan(
        linear_pair, (decay_rate, drive_term), axis=0
    )
    carried = carried_in(
        (decay_product[-1], local_states[-1]),
        "ep",
        linear_pair,
        (jnp.ones_like(decay_rate[0]), jnp.zeros_like(decay_rate[0])),
    )
    states = local_states + decay_product * carried[1][None, :]
    gated_rows = (gate_branch * states).astype(jnp.bfloat16)
    mixer_term = jnp.dot(gated_rows, out_proj, preferred_element_type=jnp.float32)
    ep_size = lax.axis_size("ep")
    local_experts = expert_gate.shape[0]
    expert_count = local_experts * ep_size
    top_count = route_ids.shape[1]
    token_count = expert_rows.shape[0]
    row_width = expert_rows.shape[1]
    capacity = token_count * top_count * 3 // (2 * expert_count)
    expert_normed = rms_scale(expert_rows, expert_gain).astype(jnp.bfloat16)
    slot_ids, source, filled = slot_table(route_ids, expert_count, capacity)
    outgoing = jnp.where(
        filled[:, None], expert_normed[source // top_count], jnp.zeros((), jnp.bfloat16)
    )
    outgoing = outgoing.reshape(ep_size, local_experts, capacity, row_width)
    received = lax.all_to_all(outgoing, "ep", split_axis=0, concat_axis=0, tiled=True)
    gate_part = jnp.einsum(
        "secd,edf->secf", received, expert_gate, preferred_element_type=jnp.float32
    )
    up_part = jnp.einsum("secd,edf->secf", received, expert_up, preferred_element_type=jnp.float32)
    copy_hidden = (jax.nn.silu(gate_part) * up_part).astype(jnp.bfloat16)
    column_sums = lax.psum_scatter(
        jnp.einsum("secf,efd->secd", copy_hidden, expert_down, preferred_element_type=jnp.float32),
        "tp",
        scatter_dimension=3,
        tiled=True,
    )
    result = lax.all_to_all(column_sums, "ep", split_axis=0, concat_axis=0, tiled=True)
    flat_back = result.reshape(expert_count * capacity, -1)
    picked = flat_back[slot_ids] * route_weights.reshape(-1, 1)
    routed = jnp.sum(picked.reshape(token_count, top_count, -1), axis=1)
    shared_hidden = (
        jax.nn.silu(jnp.dot(expert_normed, shared_gate, preferred_element_type=jnp.float32))
        * jnp.dot(expert_normed, shared_up, preferred_element_type=jnp.float32)
    ).astype(jnp.bfloat16)
    shared_term = jnp.dot(shared_hidden, shared_down, preferred_element_type=jnp.float32)
    mixer_sum, expert_sum = sent_together((mixer_term, shared_term), "tp", 0, 1)
    expert_sum = expert_sum + lax.all_to_all(routed, "tp", split_axis=0, concat_axis=1, tiled=True)
    mixer_out = rms_scale(mixer_sum, mixer_scale).astype(jnp.bfloat16)
    expert_out = rms_scale(expert_sum, expert_scale).astype(jnp.bfloat16)
    return (mixer_out, expert_out)


def solution(mesh):
    placed = (
        P("ep", None),
        P(),
        P(None, "tp"),
        P(None, "tp"),
        P(None, "tp"),
        P("tp", None, None),
        P("tp", None, None),
        P("tp"),
        P("tp", None),
        P(),
        P("ep", None),
        P(),
        P("ep", None),
        P("ep", None),
        P("ep", None, "tp"),
        P("ep", None, "tp"),
        P("ep", "tp", None),
        P(None, "tp"),
        P(None, "tp"),
        P("tp", None),
        P(),
    )
    return jax.shard_map(
        body,
        mesh=mesh,
        in_specs=placed,
        out_specs=(P(("ep", "tp"), None), P(("ep", "tp"), None)),
        check_vma=False,
    )
```

profile of v0, /device:TPU:1, one launch (start us, length us, event | category | flops | bytes accessed | tf_op | source)
XLA Modules:
  0.0 264.7 jit_solution(15755040382263902929)
XLA Ops:
  7.2 0.9 copy.64
  8.1 0.1 eq.51
  8.3 0.1 reshape.247
  8.4 2.1 fusion.7
  10.5 1.2 reduce-window.6
  11.7 0.2 slice_reduce_fusion
  12.0 0.5 convert_reduce_fusion
  12.7 2.2 fusion.9
  14.9 5.7 %gather_fusion = bf16[768,4096]{1,0:T(8,128)(2,1)} fusion(bf16[256,4096]{1,0:T(8,128)(2,1)S(1)} %fusion.9, s32[1024]{0:T(1024)S(1)} %pad_clamp_fusion.1), kind=kCustom, calls=%fused_computation | custom fusion | bytes 12585984 | tf_op jit(solution)/shard_map/gather | solution.py:166
  20.6 3.3 %broadcast_select_fusion = bf16[16,1,48,4096]{3,2,1,0:T(8,128)(2,1)S(1)} fusion(bf16[16,1,48,4096]{3,2,1,0:T(8,128)(2,1)} %bitcast.125, pred[16,48]{1,0:T(8,128)(4,1)S(1)} %gt.11), kind=kLoop, calls=%fused_computation.8 | loop fusion | flops 3145728 | bytes 12583680 | tf_op jit(solution)/shard_map/jit(_where)/select_n | solution.py:165
  23.9 80.6 %all_to_all.34 = bf16[16,1,48,4096]{3,2,1,0:T(8,128)(2,1)S(1)} all-to-all(bf16[16,1,48,4096]{3,2,1,0:T(8,128)(2,1)S(1)} %broadcast_select_fusion), channel_id=1, replica_groups=mesh['ep'=16,'tp'=8] {'ep'}, dimensions={0} | all-to-all | bytes 12582912 | tf_op jit(solution)/shard_map/all_to_all | solution.py:169
  104.5 2.6 copy-done.2
  107.1 1.8 fusion.16
  108.9 14.1 %convolution_bitcast_fusion = f32[16,1,48,4096]{3,2,0,1:T(8,128)} fusion(bf16[1,128,4096]{2,1,0:T(8,128)(2,1)S(1)} %copy-done, bf16[16,1,48,4096]{3,2,1,0:T(8,128)(2,1)} %copy-done.2, bf16[1,4096,128]{2,1,0:T(8,128)(2,1)} %param.36, f32[16,1,48,128]{3,2,0,1:T(8,128)S(1)} %fusion.16), kind=kOutput, calls=%fused_computation.3 | convolution fusion | flops 1611202560 | bytes 21364736 | tf_op jit(solution)/shard_map/secf,efd->secd/dot_general | solution.py:176
  123.1 2.1 fusion.4
  125.2 4.2 %convolution_convert_fusion = bf16[256,512]{1,0:T(8,128)(2,1)S(1)} fusion(bf16[4096,512]{1,0:T(8,128)(2,1)} %param.24, bf16[256,4096]{1,0:T(8,128)(2,1)} %param.21, f32[4096]{0:T(1024)S(1)} %copy-done.8, f32[256]{0:T(256)S(1)} %add_rsqrt_fusion.1), kind=kOutput, calls=%fused_computation.32 | convolution fusion | flops 1078067200 | bytes 6571008 | tf_op jit(solution)/shard_map/dot_general | solution.py:122
  129.4 0.6 slice.435
  130.0 2.8 %collective-permute-start = (bf16[3,512]{1,0:T(4,128)(2,1)}, bf16[3,512]{1,0:T(4,128)(2,1)}, u32[]{:S(2)}, u32[]{:S(2)}) collective-permute-start(bf16[3,512]{1,0:T(4,128)(2,1)} %slice.435), channel_id=1, source_target_pairs={{0,8},{8,16},{16,24},{24,32},{32,40},{40,48},{48,56},{56,64},{64,7... | collective-permute-start | bytes 9224 | tf_op jit(solution)/shard_map/ppermute | solution.py:13
  132.8 0.6 fusion.104
  133.4 0.6 fusion.115
  134.0 0.7 fusion.117
  134.7 4.9 %fusion.32 = f32[256,4096]{1,0:T(8,128)} fusion(bf16[128,4096]{1,0:T(8,128)(2,1)} %param.40, bf16[256,4096]{1,0:T(8,128)(2,1)S(1)} %fusion.9, bf16[4096,128]{1,0:T(8,128)(2,1)} %param.39, f32[256,128]{1,0:T(8,128)S(1)} %fusion.117), kind=kOutput, calls=%fused_computation.38 | convolution fusion | flops 537067520 | bytes 8519680 | tf_op jit(solution)/shard_map/dot_general | solution.py:189
  139.7 1.0 add_convert_fusion
  140.7 0.4 fusion.13
  141.1 0.2 copy.74
  141.3 0.4 fusion.15
  141.6 0.2 copy.75
  141.8 0.4 convert_multiply_fusion.4
  142.3 0.3 slice.337
  142.6 0.3 slice.338
  142.9 0.3 slice.336
  143.3 0.3 slice.340
  143.7 0.1 slice.343
  145.0 0.2 slice.341
  145.2 0.2 slice.390
  145.4 1.4 slice.335
  146.8 1.4 slice.392
  149.4 1.7 pad.129
  151.3 2.0 fusion.74
  153.3 0.7 pad_maximum_fusion.3
  154.0 1.1 pad.128
  155.1 1.7 pad.113
  156.8 1.0 pad_maximum_fusion.2
  157.8 1.8 pad.112
  159.5 0.7 slice_add_fusion.3
  160.3 0.7 slice_add_fusion.2
  161.0 0.6 broadcast_in_dim.44
  161.7 4.9 %all-to-all-start = ((f32[16,2,512]{2,1,0:T(2,128)}), f32[16,2,512]{2,1,0:T(2,128)S(1)}, u32[]{:S(2)}, u32[]{:S(2)}) async-start(f32[16,2,512]{2,1,0:T(2,128)} %broadcast_in_dim.44), calls=%async_computation | async-start | bytes 131072 | tf_op jit(solution)/shard_map/all_to_all | solution.py:18
  166.6 6.5 %all-to-all-done = f32[16,2,512]{2,1,0:T(2,128)S(1)} async-done(((f32[16,2,512]{2,1,0:T(2,128)}), f32[16,2,512]{2,1,0:T(2,128)S(1)}, u32[]{:S(2)}, u32[]{:S(2)}) %all-to-all-start) | async-done | bytes 65568 | tf_op jit(solution)/shard_map/all_to_all | solution.py:18
  173.5 8.6 %fusion.59 = f32[256,4096]{1,0:T(8,128)} fusion(bf16[512,4096]{1,0:T(8,128)(2,1)} %param.29, bf16[4096,512]{1,0:T(8,128)(2,1)} %param.23, bf16[256,4096]{1,0:T(8,128)(2,1)S(1)} %copy-done.3, f32[4096]{0:T(1024)S(1)} %copy-done.9, f32[256]{0:T(256)S(1)} %copy-done.15, f32[256,512]{1,0:T(8,128)S(1)} %pad.128, f32[256,512]{1,0:T(8,128)S(1)} %copy-done.4, ...), kind=kOutput, calls=%fused_computation.54 | convolution fusion | flops 2153512960 | bytes 16796672 | tf_op jit(solution)/shard_map/dot_general | solution.py:155
  182.1 7.7 %pad_maximum_fusion = f32[256,8192]{1,0:T(8,128)} fusion(f32[256,4096]{1,0:T(8,128)} %fusion.32, f32[256,4096]{1,0:T(8,128)} %fusion.59), kind=kLoop, calls=%fused_computation.2 | loop fusion | flops 2097152 | bytes 16777216 | tf_op jit(solution)/shard_map/concatenate | solution.py:63
  189.9 4.3 %reduce-scatter.5.cloned.1.call-done = f32[16,1,48,512]{3,2,0,1:T(8,128)} async-done(((f32[16,1,48,4096]{3,2,0,1:T(8,128)}), f32[16,1,48,512]{3,2,0,1:T(8,128)}) %reduce-scatter.5.cloned.1.call-update) | async-done | bytes 1572880 | tf_op jit(solution)/shard_map/reduce_scatter | solution.py:175
  194.1 6.7 %all-to-all-start.2 = ((f32[16,1,48,512]{3,2,1,0:T(8,128)}), f32[16,1,48,512]{3,2,1,0:T(8,128)S(1)}, u32[]{:S(2)}, u32[]{:S(2)}) async-start(f32[16,1,48,512]{3,2,1,0:T(8,128)} %bitcast.130), calls=%async_computation.4 | async-start | bytes 3145728 | tf_op jit(solution)/shard_map/all_to_all | solution.py:181
  200.8 0.1 copy.69
  201.0 0.1 mul.443
  201.1 0.1 copy.70
  201.3 20.8 %all-to-all-done.2 = f32[16,1,48,512]{3,2,1,0:T(8,128)S(1)} async-done(((f32[16,1,48,512]{3,2,1,0:T(8,128)}), f32[16,1,48,512]{3,2,1,0:T(8,128)S(1)}, u32[]{:S(2)}, u32[]{:S(2)}) %all-to-all-start.2) | async-done | bytes 1572896 | tf_op jit(solution)/shard_map/all_to_all | solution.py:181
  222.1 2.3 gather_fusion.1
  224.4 2.0 gather.13
  226.4 1.3 multiply_reduce_fusion
  227.7 22.3 %all_to_all.35 = f32[8,32,512]{2,1,0:T(8,128)S(1)} all-to-all(f32[8,32,512]{2,1,0:T(8,128)S(1)} %bitcast.128), channel_id=1, replica_groups=mesh['ep'=16,'tp'=8] {'tp'}, dimensions={0} | all-to-all | bytes 1048576 | tf_op jit(solution)/shard_map/all_to_all | solution.py:191
  250.1 4.2 %reduce-scatter.3.cloned.1.call-done = f32[32,8192]{1,0:T(8,128)} async-done(((f32[256,8192]{1,0:T(8,128)}), f32[32,8192]{1,0:T(8,128)}) %reduce-scatter.3.cloned.1.call-update) | async-done | bytes 1048592 | tf_op jit(solution)/shard_map/reduce_scatter | solution.py:64
  254.3 1.4 multiply_reduce_fusion.1
  255.7 2.2 multiply_convert_fusion
  (189 shorter events, 3.1 us)
Async XLA Ops:
  7.2 101.7 %copy-start = (bf16[1,128,4096]{2,1,0:T(8,128)(2,1)S(1)}, bf16[1,128,4096]{2,1,0:T(8,128)(2,1)}, u32[]{:S(2)}) copy-start(bf16[1,128,4096]{2,1,0:T(8,128)(2,1)} %param.37) | copy-start | bytes 3145732
  7.2 187.0 %reduce-scatter.5.cloned.1.call-start = ((), (), s32[]{:S(2)}) async-start(), calls=%async_computation.7 | async-start | bytes 14155776 | tf_op jit(solution)/shard_map/reduce_scatter | solution.py:175
  23.9 83.2 %copy-start.18 = (bf16[1,4096,128]{2,1,0:T(8,128)(2,1)S(1)}, bf16[1,4096,128]{2,1,0:T(8,128)(2,1)}, u32[]{:S(2)}) copy-start(bf16[1,4096,128]{2,1,0:T(8,128)(2,1)} %param.35) | copy-start | bytes 3145732
  104.5 2.6 copy-start.2
  123.0 2.1 copy-start.8
  125.2 4.3 %copy-start.14 = (f32[256]{0:T(256)}, f32[256]{0:T(256)S(1)}, u32[]{:S(2)}) copy-start(f32[256]{0:T(256)S(1)} %add_rsqrt_fusion.1) | copy-start | bytes 3076
  125.2 7.6 %copy-start.17 = (f32[512]{0:T(512)S(1)}, f32[512]{0:T(512)}, u32[]{:S(2)}) copy-start(f32[512]{0:T(512)} %param.28) | copy-start | bytes 6148
  125.2 8.2 %copy-start.12 = (f32[4,512]{1,0:T(4,128)S(1)}, f32[4,512]{1,0:T(4,128)}, u32[]{:S(2)}) copy-start(f32[4,512]{1,0:T(4,128)} %param.25) | copy-start | bytes 24580
  125.2 8.8 %copy-start.5 = (bf16[4096,128]{1,0:T(8,128)(2,1)S(1)}, bf16[4096,128]{1,0:T(8,128)(2,1)}, u32[]{:S(2)}) copy-start(bf16[4096,128]{1,0:T(8,128)(2,1)} %param.38) | copy-start | bytes 3145732
  130.0 9.6 %collective-permute-start = (bf16[3,512]{1,0:T(4,128)(2,1)}, bf16[3,512]{1,0:T(4,128)(2,1)}, u32[]{:S(2)}, u32[]{:S(2)}) collective-permute-start(bf16[3,512]{1,0:T(4,128)(2,1)} %slice.435), channel_id=1, source_target_pairs={{0,8},{8,16},{16,24},{24,32},{32,40},{40,48},{48,56},{56,64},{64,7... | collective-permute-start | bytes 9224 | tf_op jit(solution)/shard_map/ppermute | solution.py:13
  134.7 4.9 %copy-start.11 = (f32[1,512]{1,0:T(1,128)S(1)}, f32[1,512]{1,0:T(1,128)}, u32[]{:S(2)}) copy-start(f32[1,512]{1,0:T(1,128)} %get-tuple-element.47) | copy-start | bytes 6148
  134.7 6.0 %copy-start.19 = (bf16[2,256,256]{2,1,0:T(8,128)(2,1)S(1)}, bf16[2,256,256]{2,1,0:T(8,128)(2,1)}, u32[]{:S(2)}) copy-start(bf16[2,256,256]{2,1,0:T(8,128)(2,1)} %param.27) | copy-start | bytes 786436
  139.6 1.6 copy-start.20
  139.6 2.2 copy-start.13
  151.1 22.4 %copy-start.3 = (bf16[256,4096]{1,0:T(8,128)(2,1)S(1)}, bf16[256,4096]{1,0:T(8,128)(2,1)}, u32[]{:S(2)}) copy-start(bf16[256,4096]{1,0:T(8,128)(2,1)} %param.21) | copy-start | bytes 6291460
  151.1 22.4 %copy-start.9 = (f32[4096]{0:T(1024)S(1)}, f32[4096]{0:T(1024)}, u32[]{:S(2)}) copy-start(f32[4096]{0:T(1024)} %param.22) | copy-start | bytes 49156
  151.1 22.4 %copy-start.15 = (f32[256]{0:T(256)S(1)}, f32[256]{0:T(256)}, u32[]{:S(2)}) copy-start(f32[256]{0:T(256)} %copy-done.14) | copy-start | bytes 3076
  153.3 20.2 %copy-start.4 = (f32[256,512]{1,0:T(8,128)S(1)}, f32[256,512]{1,0:T(8,128)}, u32[]{:S(2)}) copy-start(f32[256,512]{1,0:T(8,128)} %pad.129) | copy-start | bytes 1572868
  161.7 11.4 %all-to-all-start = ((f32[16,2,512]{2,1,0:T(2,128)}), f32[16,2,512]{2,1,0:T(2,128)S(1)}, u32[]{:S(2)}, u32[]{:S(2)}) async-start(f32[16,2,512]{2,1,0:T(2,128)} %broadcast_in_dim.44), calls=%async_computation | async-start | bytes 131072 | tf_op jit(solution)/shard_map/all_to_all | solution.py:18
  166.5 87.7 %reduce-scatter.3.cloned.1.call-start = ((), (), s32[]{:S(2)}) async-start(), calls=%async_computation.6 | async-start | bytes 9437184 | tf_op jit(solution)/shard_map/reduce_scatter | solution.py:64
  189.8 11.0 %copy-start.10 = (s32[256,2]{0,1:T(2,128)S(1)}, s32[256,2]{0,1:T(2,128)}, u32[]{:S(2)}) copy-start(s32[256,2]{0,1:T(2,128)} %param.33) | copy-start | bytes 6148
  189.8 11.3 %copy-start.16 = (f32[256,2]{0,1:T(2,128)S(1)}, f32[256,2]{0,1:T(2,128)}, u32[]{:S(2)}) copy-start(f32[256,2]{0,1:T(2,128)} %param.34) | copy-start | bytes 6148
  194.1 27.9 %all-to-all-start.2 = ((f32[16,1,48,512]{3,2,1,0:T(8,128)}), f32[16,1,48,512]{3,2,1,0:T(8,128)S(1)}, u32[]{:S(2)}, u32[]{:S(2)}) async-start(f32[16,1,48,512]{3,2,1,0:T(8,128)} %bitcast.130), calls=%async_computation.4 | async-start | bytes 3145728 | tf_op jit(solution)/shard_map/all_to_all | solution.py:181
  224.4 31.3 %copy-start.6 = (f32[4096]{0:T(1024)S(1)}, f32[4096]{0:T(1024)}, u32[]{:S(2)}) copy-start(f32[4096]{0:T(1024)} %param.41) | copy-start | bytes 49156
  224.4 31.3 %copy-start.7 = (f32[4096]{0:T(1024)S(1)}, f32[4096]{0:T(1024)}, u32[]{:S(2)}) copy-start(f32[4096]{0:T(1024)} %param.30) | copy-start | bytes 49156
  224.4 33.5 %copy-start.1 = (bf16[1,128,4096]{2,1,0:T(8,128)(2,1)S(1)}, bf16[1,128,4096]{2,1,0:T(8,128)(2,1)}, u32[]{:S(2)}) copy-start(bf16[1,128,4096]{2,1,0:T(8,128)(2,1)} %param.37) | copy-start | bytes 3145732
Sparse Core Ops, SparseCore 0:
  123.2 70.9 reduce-scatter.4
  196.5 57.6 reduce-scatter.2
where the time goes:
time: 265 us
  blocking collectives  103 us (39%)
  waiting for transfers between devices  35.7 us (13%)
  matrix products  35 us (13%)
  other arithmetic  32.2 us (12%)
  local copies, waits for them, and re-layouts  29.4 us (11%)
  between operations  15.1 us (6%)
  starting transfers between devices  14.4 us (5%)
    all_to_all x1, blocking collectives, body(): lax.all_to_all(outgoing, 'ep', split_axis=0, concat_axis=0, tiled=True)  80.6 us
    all_to_all x1, blocking collectives, body(): lax.all_to_all(routed, 'tp', split_axis=0, concat_axis=1, tiled=True)  22.3 us
    all_to_all x1, waiting for transfers between devices, body(): lax.all_to_all(column_sums, 'ep', split_axis=0, concat_axis=0, tiled=True)  20.8 us
    dot_general x1, matrix products, body(): jnp.einsum('secf,efd->secd', copy_hidden, expert_down, preferred_element_...  14.1 us
    dot_general x1, matrix products, body(): jnp.dot(gated_rows, out_proj, preferred_element_type=jnp.float32)  8.58 us
    concatenate x1, other arithmetic, sent_together(): both = jnp.concatenate(arrays, axis=along)  7.72 us
    all_to_all x1, starting transfers between devices, body(): lax.all_to_all(column_sums, 'ep', split_axis=0, concat_axis=0, tiled=True)  6.68 us
    pad x28, local copies, waits for them, and re-layouts, body(): lax.associative_scan(linear_pair, (decay_rate, drive_term), axis=0)  6.67 us
  transfers between devices with their start and end apart: 5, of which 4 were waited for; matrix products, arithmetic and copies ran while one was open for 22% of the time, Pallas kernels for 0%

commit v1 on v0

v1 whole, which is shorter than its diff:
```python
import functools

import jax
import jax.numpy as jnp
from jax import lax
from jax.experimental import pallas as pl
from jax.experimental.pallas import tpu as pltpu
from jax.sharding import PartitionSpec as P


eps = 1e-06
lru_power = 8.0
bf16 = jnp.bfloat16
f32 = jnp.float32


def vmem():
    return pl.BlockSpec(memory_space=pltpu.VMEM)


def smem():
    return pl.BlockSpec(memory_space=pltpu.SMEM)


def hbm():
    return pl.BlockSpec(memory_space=pltpu.HBM)


def params(mib, micros):
    return dict(
        compiler_params=pltpu.CompilerParams(vmem_limit_bytes=mib * 2**20),
        cost_estimate=pl.CostEstimate(
            flops=int(micros * 1e9), transcendentals=0, bytes_accessed=int(micros * 1e6)
        ),
    )


def normed_block(rows, gain):
    floats = rows.astype(f32)
    return floats * lax.rsqrt(jnp.mean(floats * floats, axis=-1, keepdims=True) + eps) * gain


def norm_part(src, gain, dst, take, put, count, step):
    def one(i, _):
        start = i * step
        dst[pl.ds(pl.multiple_of(put + start, 8), step), :] = normed_block(
            src[pl.ds(pl.multiple_of(take + start, step), step), :], gain
        ).astype(bf16)
        return 0

    lax.fori_loop(0, count // step, one, 0)


def minus_expm1(v):
    series = jnp.ones_like(v)
    for n in (8, 7, 6, 5, 4, 3, 2):
        series = 1.0 + series * v * (1.0 / n)
    return jnp.where(v > -0.35, -v * series, 1.0 - jnp.exp(v))


def mixer_kernel(
    first, rows_hbm, halo, gain, gate_hbm, input_hbm, taps, in_gates, de_gates, offset,
    gate_out, states_out, decay_out, carry_out, rows, normed, weights, sems,
):
    count = rows.shape[0]
    pieces = 4
    part = count // pieces
    loads = [
        pltpu.make_async_copy(
            rows_hbm.at[k * part : (k + 1) * part, :], rows.at[k * part : (k + 1) * part, :], sems.at[k]
        )
        for k in range(pieces)
    ]
    copies = [
        pltpu.make_async_copy(src, weights.at[k], sems.at[pieces + k])
        for k, src in enumerate((input_hbm, gate_hbm))
    ]
    for c in loads + copies:
        c.start()
    pad = halo.shape[0]
    gains = gain[...]
    normed[0:pad, :] = normed_block(halo[...], gains).astype(bf16)
    for k in range(pieces):
        loads[k].wait()
        norm_part(rows, gains, normed, k * part, pad + k * part, part, 16)
    copies[0].wait()
    branch = jnp.dot(normed[...], weights[0], preferred_element_type=f32).astype(bf16).astype(f32)
    tap_count = taps.shape[0]
    conv = None
    for k in range(tap_count):
        back = tap_count - 1 - k
        moved = pltpu.roll(branch, back, 0) if back else branch
        term = taps[k : k + 1, :] * moved
        conv = term if conv is None else conv + term
    conv = conv[pad:, :].astype(bf16)
    width = in_gates.shape[1]
    blocks = in_gates.shape[0]

    def gate(maps):
        return jax.nn.sigmoid(
            jnp.concatenate(
                [
                    jnp.dot(conv[:, b * width : (b + 1) * width], maps[b], preferred_element_type=f32)
                    for b in range(blocks)
                ],
                axis=1,
            )
        )

    input_gate = gate(in_gates)
    decay_gate = gate(de_gates)
    minus_offset = -offset[...]
    softplus = jnp.maximum(minus_offset, 0.0) + jnp.log1p(jnp.exp(-jnp.abs(minus_offset)))
    log_decay = -lru_power * decay_gate * softplus
    row_ids = lax.broadcasted_iota(jnp.int32, log_decay.shape, 0)
    scale = jnp.sqrt(minus_expm1(2.0 * log_decay))
    scale = jnp.where((row_ids == 0) & (first[2] == 0), 1.0, scale)
    state = scale * input_gate * conv.astype(f32)
    decay = jnp.exp(log_decay)
    step = 1
    while step < count:
        keep = row_ids >= step
        before_state = jnp.where(keep, pltpu.roll(state, step, 0), 0.0)
        before_decay = jnp.where(keep, pltpu.roll(decay, step, 0), 1.0)
        state = decay * before_state + state
        decay = decay * before_decay
        step *= 2
    states_out[...] = state
    decay_out[...] = decay
    carry_out[0:1, :] = decay[count - 1 :, :]
    carry_out[1:2, :] = state[count - 1 :, :]
    copies[1].wait()
    gate_out[...] = jax.nn.gelu(
        jnp.dot(normed[pad:, :], weights[1], preferred_element_type=f32)
    )


def mixer_local(first, rows, halo, gain, gate_proj, input_proj, taps, in_gates, de_gates, offset):
    count, width = rows.shape[0], gate_proj.shape[1]
    full = jax.ShapeDtypeStruct((count, width), f32)
    return pl.pallas_call(
        mixer_kernel,
        out_shape=(full, full, full, jax.ShapeDtypeStruct((2, width), f32)),
        in_specs=[smem(), hbm(), vmem(), vmem(), hbm(), hbm(), vmem(), vmem(), vmem(), vmem()],
        out_specs=(vmem(), vmem(), vmem(), vmem()),
        scratch_shapes=[
            pltpu.VMEM(rows.shape, bf16),
            pltpu.VMEM((count + halo.shape[0], rows.shape[1]), bf16),
            pltpu.VMEM((2, *gate_proj.shape), bf16),
            pltpu.SemaphoreType.DMA((6,)),
        ],
        name="mixer_local",
        **params(24, 8),
    )(first, rows, halo, gain, gate_proj, input_proj, taps, in_gates, de_gates, offset)


def front_kernel(
    core, rows_hbm, gain, ids, mixer_hbm, out_hbm, normed_hbm, slots, tail,
    rows, normed, out, sems, *, experts, capacity,
):
    count, _ = rows.shape
    half = out.shape[1]
    pieces = 4
    part = count // pieces
    loads = [
        pltpu.make_async_copy(
            rows_hbm.at[k * part : (k + 1) * part, :], rows.at[k * part : (k + 1) * part, :], sems.at[k]
        )
        for k in range(pieces)
    ]
    last = mixer_hbm.shape[0]
    loads.append(pltpu.make_async_copy(mixer_hbm.at[last - 8 : last, :], tail, sems.at[pieces]))
    for c in loads:
        c.start()
    experts_down = lax.broadcasted_iota(jnp.int32, (experts, count), 0)
    picks = [ids[k : k + 1, :] for k in range(2)]
    hits = [(p == experts_down) for p in picks]
    marks = jnp.where(hits[0] | hits[1], 1.0, 0.0).astype(bf16)
    upper = jnp.where(
        lax.broadcasted_iota(jnp.int32, (count, count), 0)
        < lax.broadcasted_iota(jnp.int32, (count, count), 1),
        1.0,
        0.0,
    ).astype(bf16)
    earlier = jnp.dot(marks, upper, preferred_element_type=f32)
    slots_down = lax.broadcasted_iota(jnp.int32, (experts * capacity, count), 0)
    chosen = None
    for k in range(2):
        place = jnp.sum(jnp.where(hits[k], earlier, 0.0), axis=0, keepdims=True).astype(jnp.int32)
        slot = picks[k] * capacity + place
        slots[k : k + 1, :] = slot
        hit = slot == slots_down
        chosen = hit if chosen is None else chosen | hit
    chosen = jnp.where(chosen, 1.0, 0.0).astype(bf16)
    gains = gain[...]
    saves = []
    for k in range(pieces):
        loads[k].wait()
        norm_part(rows, gains, normed, k * part, k * part, part, 16)
        save = pltpu.make_async_copy(
            normed.at[k * part : (k + 1) * part, :],
            normed_hbm.at[k * part : (k + 1) * part, :],
            sems.at[5 + k],
        )
        save.start()
        saves.append(save)
    mine = normed[:, pl.ds(pl.multiple_of(core[0] * half, half), half)]
    blocks = 3
    size = experts * capacity // blocks
    for k in range(blocks):
        out[k * size : (k + 1) * size, :] = jnp.dot(
            chosen[k * size : (k + 1) * size, :], mine, preferred_element_type=f32
        ).astype(bf16)
        save = pltpu.make_async_copy(
            out.at[k * size : (k + 1) * size, :], out_hbm.at[k * size : (k + 1) * size, :], sems.at[9 + k]
        )
        save.start()
        saves.append(save)
    loads[pieces].wait()
    for c in saves:
        c.wait()


def expert_front(core, rows, gain, ids, mixer_rows, experts, capacity):
    count, width = rows.shape
    return pl.pallas_call(
        functools.partial(front_kernel, experts=experts, capacity=capacity),
        out_shape=(
            jax.ShapeDtypeStruct((experts * capacity, width // 2), bf16),
            jax.ShapeDtypeStruct((count, width), bf16),
            jax.ShapeDtypeStruct((2, count), jnp.int32),
            jax.ShapeDtypeStruct((8, width), bf16),
        ),
        in_specs=[smem(), hbm(), vmem(), vmem(), hbm()],
        out_specs=(hbm(), hbm(), vmem(), vmem()),
        scratch_shapes=[
            pltpu.VMEM((count, width), bf16),
            pltpu.VMEM((count, width), bf16),
            pltpu.VMEM((experts * capacity, width // 2), bf16),
            pltpu.SemaphoreType.DMA((12,)),
        ],
        name="expert_front",
        **params(20, 5),
    )(core, rows, gain, ids, mixer_rows)


def parts_kernel(core, received_hbm, gate, up, out, received, weights, sems, *, whole):
    half, width = weights.shape[0], gate.shape[1]
    start = pl.multiple_of(core[0] * half, half) if whole else 0
    copies = [
        pltpu.make_async_copy(
            src.at[pl.ds(start, half), :], weights.at[:, k * width : (k + 1) * width], sems.at[k]
        )
        for k, src in enumerate((gate, up))
    ]
    pieces = 3
    part = received.shape[0] // pieces
    loads = [
        pltpu.make_async_copy(
            received_hbm.at[k * part : (k + 1) * part, :],
            received.at[k * part : (k + 1) * part, :],
            sems.at[2 + k],
        )
        for k in range(pieces)
    ]
    for c in copies + loads:
        c.start()
    for c in copies:
        c.wait()
    for k in range(pieces):
        loads[k].wait()
        out[k * part : (k + 1) * part, :] = jnp.dot(
            received[k * part : (k + 1) * part, :], weights[...], preferred_element_type=f32
        )


def expert_parts(core, received, gate, up, whole):
    rows, half = received.shape
    width = gate.shape[1]
    return pl.pallas_call(
        functools.partial(parts_kernel, whole=whole),
        out_shape=jax.ShapeDtypeStruct((rows, 2 * width), f32),
        in_specs=[smem(), hbm(), hbm(), hbm()],
        out_specs=vmem(),
        scratch_shapes=[
            pltpu.VMEM(received.shape, bf16),
            pltpu.VMEM((half, 2 * width), bf16),
            pltpu.SemaphoreType.DMA((5,)),
        ],
        name="expert_parts",
        **params(8, 3),
    )(core, received, gate, up)


def prep_kernel(where, gate, up, down, shared, gate_out, up_out, *refs):
    outs, sems = refs[:4], refs[4]
    half, quarter = gate_out.shape[0], outs[0].shape[1]
    size = down.shape[0]
    start = pl.multiple_of((1 - where[0]) * half, half)
    copies = [
        pltpu.make_async_copy(src.at[pl.ds(start, half), :], dst, sems.at[k])
        for k, (src, dst) in enumerate(((gate, gate_out), (up, up_out)))
    ]
    for s in range(4):
        cols = pl.ds(pl.multiple_of(((where[1] + s) % 4) * quarter, quarter), quarter)
        for k, src in enumerate((down, shared)):
            copies.append(
                pltpu.make_async_copy(
                    src.at[:, cols], outs[s].at[k * size : (k + 1) * size, :], sems.at[2 + 2 * s + k]
                )
            )
    for c in copies:
        c.start()
    for c in copies:
        c.wait()


def prepared(where, gate, up, down, shared):
    half, width = gate.shape[0] // 2, gate.shape[1]
    tall = jax.ShapeDtypeStruct((half, width), bf16)
    wide = jax.ShapeDtypeStruct((2 * down.shape[0], down.shape[1] // 4), bf16)
    return pl.pallas_call(
        prep_kernel,
        out_shape=(tall, tall, wide, wide, wide, wide),
        in_specs=[smem()] + [hbm()] * 4,
        out_specs=(hbm(),) * 6,
        scratch_shapes=[pltpu.SemaphoreType.DMA((10,))],
        name="prepared",
        **params(2, 3),
    )(where, gate, up, down, shared)


def down_kernel(core, *refs, at):
    hidden, weights, (keep, send, w, sems) = refs[:4], refs[4:8], refs[8:]
    size = hidden[0].shape[1]
    width = keep.shape[1]
    copies = [
        pltpu.make_async_copy(
            p.at[at : at + size, :], w.at[k * size : (k + 1) * size, :], sems.at[k]
        )
        for k, p in enumerate(weights)
    ]
    for c in copies:
        c.start()
    h = jnp.concatenate([p[...] for p in hidden], axis=1)
    for c in copies:
        c.wait()
    for out, which in ((send, 1 - core[0]), (keep, core[0])):
        cols = pl.ds(pl.multiple_of(which * width, width), width)
        out[...] = jnp.dot(h, w[:, cols], preferred_element_type=f32)


def down_parts(core, hidden, weights, at):
    width = weights[0].shape[1] // 2
    shape = jax.ShapeDtypeStruct((hidden[0].shape[0], width), f32)
    return pl.pallas_call(
        functools.partial(down_kernel, at=at),
        out_shape=(shape, shape),
        in_specs=[smem()] + [vmem()] * 4 + [hbm()] * 4,
        out_specs=(vmem(), vmem()),
        scratch_shapes=[
            pltpu.VMEM((4 * hidden[0].shape[1], 2 * width), bf16),
            pltpu.SemaphoreType.DMA((4,)),
        ],
        name="down_parts",
        **params(10, 2.5),
    )(core, *hidden, *weights)


def mixer_out_kernel(where, gate, states, decays, carries, out_hbm, keep, send, gated, weights, sem):
    load = pltpu.make_async_copy(out_hbm, weights, sem)
    load.start()
    carried = jnp.zeros((1, gate.shape[1]), f32)
    for i in range(carries.shape[0] - 1):
        carried = jnp.where(i < where[2], carries[i, 0:1] * carried + carries[i, 1:2], carried)
    gated[...] = (gate[...] * (states[...] + decays[...] * carried)).astype(bf16)
    rows = keep.shape[0] // 4
    load.wait()
    for out, which in ((send, 1 - where[0]), (keep, where[0])):
        picked = jnp.concatenate(
            [
                gated[pl.ds(pl.multiple_of((2 * i + which) * rows, rows), rows), :]
                for i in range(4)
            ],
            axis=0,
        )
        out[...] = jnp.dot(picked, weights[...], preferred_element_type=f32)


def mixer_out_parts(where, gate, states, decays, carries, out_proj):
    rows, width = gate.shape[0], out_proj.shape[1]
    shape = jax.ShapeDtypeStruct((rows // 2, width), f32)
    return pl.pallas_call(
        mixer_out_kernel,
        out_shape=(shape, shape),
        in_specs=[smem()] + [vmem()] * 4 + [hbm()],
        out_specs=(vmem(), vmem()),
        scratch_shapes=[
            pltpu.VMEM(gate.shape, bf16),
            pltpu.VMEM(out_proj.shape, bf16),
            pltpu.SemaphoreType.DMA,
        ],
        name="mixer_out",
        **params(16, 3),
    )(where, gate, states, decays, carries, out_proj)


def combine_kernel(back, slots, weights, own, other, out):
    down = lax.broadcasted_iota(jnp.int32, (back.shape[0], slots.shape[1]), 0)
    mix = jnp.where(slots[0:1, :] == down, weights[0:1, :], 0.0) + jnp.where(
        slots[1:2, :] == down, weights[1:2, :], 0.0
    )
    out[...] = own[...] + other[...] + lax.dot_general(
        mix, back[...], (((0,), (0,)), ((), ())), preferred_element_type=f32,
        precision=lax.Precision.HIGHEST,
    )


def combined(back, slots, weights, own, other):
    return pl.pallas_call(
        combine_kernel,
        out_shape=jax.ShapeDtypeStruct(own.shape, f32),
        in_specs=[vmem()] * 5,
        out_specs=vmem(),
        name="combine",
        **params(12, 3),
    )(back, slots, weights, own, other)


def rms_scale(values, scale):
    return values * lax.rsqrt(jnp.mean(values * values, axis=-1, keepdims=True) + eps) * scale


def swapped(block):
    return lax.ppermute(block, "tp", [(i, i ^ 1) for i in range(8)])


def turned(block, by):
    return lax.ppermute(block, "tp", [(i, (i + 2 * by) % 8) for i in range(8)])


def after(value, *others):
    return lax.optimization_barrier((value, *others))[0]


def gathered(block):
    return [block] + [turned(block, s) for s in (1, 3, 2)]


def whole_body(
    mixer_rows, mixer_gain, gate_proj, input_proj, conv_taps, input_gates, decay_gates,
    decay_offset, out_proj, mixer_scale, expert_rows, expert_gain, route_ids, route_weights,
    expert_gate, expert_up, expert_down, shared_gate, shared_up, shared_down, expert_scale,
):
    ep_index, tp_index = lax.axis_index("ep"), lax.axis_index("tp")
    core, chip = tp_index % 2, tp_index // 2
    where = jnp.stack([core, chip, ep_index])
    rows, width = mixer_rows.shape
    experts = lax.axis_size("ep")
    capacity = rows * 2 * 3 // (2 * experts)
    half = width // 2
    order = (1, 3, 2)

    outgoing, expert_normed, slots, tail = expert_front(
        where, expert_rows, expert_gain.reshape(1, -1), route_ids.T, mixer_rows, experts, capacity
    )
    halo = lax.ppermute(tail, "ep", [(i, i + 1) for i in range(15)])
    received = lax.all_to_all(
        outgoing.reshape(experts, capacity, half), "ep", 0, 0, tiled=True
    ).reshape(experts * capacity, half)

    send_gate, send_up, *downs = prepared(
        after(where, slots), expert_gate[0], expert_up[0], expert_down[0], shared_down
    )
    shared_hidden = (
        jax.nn.silu(jnp.dot(expert_normed, shared_gate, preferred_element_type=f32))
        * jnp.dot(expert_normed, shared_up, preferred_element_type=f32)
    ).astype(bf16)
    shared_all = gathered(shared_hidden)
    other_gate, other_up = (swapped(w) for w in (send_gate, send_up))
    downs = [downs[0]] + [turned(downs[s], s) for s in order]

    gate_branch, local_states, decay_product, carry = mixer_local(
        after(where, shared_hidden, send_gate), mixer_rows, halo, mixer_gain.reshape(1, -1), gate_proj, input_proj,
        conv_taps, input_gates, decay_gates, decay_offset.reshape(1, -1),
    )
    hidden_width = expert_gate.shape[2]
    shared_keep, shared_send = down_parts(after(where, carry), shared_all, downs, hidden_width)
    shared_other = swapped(shared_send)

    received = after(received, carry, shared_keep, other_gate, other_up)
    other_part = expert_parts(where, received, other_gate, other_up, False)
    own_part = expert_parts(where, received, expert_gate[0], expert_up[0], True)
    parts = own_part + swapped(other_part)
    copy_hidden = (jax.nn.silu(parts[:, :hidden_width]) * parts[:, hidden_width:]).astype(bf16)
    hidden_all = gathered(copy_hidden)
    carry = after(carry, copy_hidden)
    carries = lax.all_to_all(jnp.broadcast_to(carry[None], (experts, *carry.shape)), "ep", 0, 0, tiled=True)
    keep_result, send_result = down_parts(where, hidden_all, downs, 0)
    results = keep_result + swapped(send_result)
    back = lax.all_to_all(
        results.reshape(experts, capacity, -1), "ep", 0, 0, tiled=True
    ).reshape(experts * capacity, -1)

    carries = after(carries, keep_result)
    keep_term, send_term = mixer_out_parts(where, gate_branch, local_states, decay_product, carries, out_proj)
    pair_term = (keep_term + swapped(send_term)).reshape(4, rows // 8, width)
    mixer_sum = lax.dynamic_index_in_dim(pair_term, chip, 0, keepdims=False)
    for s in order:
        mixer_sum = mixer_sum + turned(
            lax.dynamic_index_in_dim(pair_term, (chip + s) % 4, 0, keepdims=False).astype(bf16), s
        ).astype(f32)
    mixer_out = rms_scale(mixer_sum, mixer_scale).astype(bf16)

    expert_sum = combined(back, slots, route_weights.T, shared_keep, shared_other)
    expert_whole = lax.all_to_all(expert_sum, "tp", split_axis=0, concat_axis=1, tiled=True)
    expert_out = rms_scale(expert_whole, expert_scale).astype(bf16)
    return (mixer_out, expert_out)


def solution(mesh):
    placed = (
        P("ep", None), P(), P(None, "tp"), P(None, "tp"), P(None, "tp"), P("tp", None, None),
        P("tp", None, None), P("tp"), P("tp", None), P(), P("ep", None), P(), P("ep", None),
        P("ep", None), P("ep", None, "tp"), P("ep", None, "tp"), P("ep", "tp", None),
        P(None, "tp"), P(None, "tp"), P("tp", None), P(),
    )
    return jax.shard_map(
        whole_body,
        mesh=mesh,
        in_specs=placed,
        out_specs=(P(("ep", "tp"), None), P(("ep", "tp"), None)),
        check_vma=False,
    )
```

time: 265 us -> 194 us (0.73)
  blocking collectives: 103 us -> 0 us
  starting transfers between devices: 14.4 us -> 59.4 us
  matrix products: 35 us -> 1.47 us
  Pallas kernels: 0 us -> 33.1 us
  waiting for transfers between devices: 35.7 us -> 68.4 us
  other arithmetic: 32.2 us -> 7.97 us
  between operations: 15.1 us -> 1.29 us
  local copies, waits for them, and re-layouts: 29.4 us -> 21.6 us
    all_to_all x2 -> x0, blocking collectives: 103 us -> none  [the longest x1 80.6 us: body(): lax.all_to_all(outgoing, 'ep', split_axis=0, concat_axis=0, tiled=True)]
    ppermute x1 -> x19, waiting for transfers between devices: 0.01 us -> 54.7 us  [the longest x1 28.7 us: whole_body(): halo = lax.ppermute(tail, 'ep', [(i, i + 1) for i in range(15)])]
    dot_general x8 -> x2, matrix products: 35 us -> 1.47 us  [the longest x1 0.75 us: whole_body(): jnp.dot(expert_normed, shared_gate, preferred_element_type=f32)]
    pallas_call x0 -> x9, Pallas kernels: none -> 33.1 us  [the longest x1 8.53 us: mixer_local(): pl.pallas_call(mixer_kernel, out_shape=(full, full, full, jax.ShapeDtypeS...]
    ppermute x1 -> x19, starting transfers between devices: 2.78 us -> 29.7 us  [the longest x12 15.6 us: turned(): return lax.ppermute(block, 'tp', [(i, (i + 2 * by) % 8) for i in range(8)])]
    all_to_all x2 -> x4, starting transfers between devices: 11.6 us -> 29.6 us  [the longest x1 9.38 us: whole_body(): lax.all_to_all(jnp.broadcast_to(carry[None], (experts, *carry.shape)), 'e...]
    unnamed x44 -> x96, local copies, waits for them, and re-layouts: 3.72 us -> 20.1 us
    all_to_all x2 -> x4, waiting for transfers between devices: 27.2 us -> 13.7 us  [the longest x1 7.46 us: whole_body(): lax.all_to_all(expert_sum, 'tp', split_axis=0, concat_axis=1, tiled=True)]
  transfers between devices with their start and end apart: 5 -> 23, of which waited for: 4 -> 9; matrix products, arithmetic and copies ran while one was open for 22% -> 5% of each run, Pallas kernels for 0% -> 9%
where the time goes in v1:
time: 194 us; the launch traced here: 193 us
  waiting for transfers between devices  68.4 us (35%)
  starting transfers between devices  59.4 us (31%)
  Pallas kernels  33.1 us (17%)
  local copies, waits for them, and re-layouts  21.6 us (11%)
  other arithmetic  7.97 us (4%)
    ppermute x1, waiting for transfers between devices, whole_body(): halo = lax.ppermute(tail, 'ep', [(i, i + 1) for i in range(15)])  28.7 us
    unnamed x96, local copies, waits for them, and re-layouts  20.1 us
    ppermute x12, waiting for transfers between devices, turned(): return lax.ppermute(block, 'tp', [(i, (i + 2 * by) % 8) for i in range(8)])  19.9 us
    ppermute x12, starting transfers between devices, turned(): return lax.ppermute(block, 'tp', [(i, (i + 2 * by) % 8) for i in range(8)])  15.6 us
    ppermute x6, starting transfers between devices, swapped(): return lax.ppermute(block, 'tp', [(i, i ^ 1) for i in range(8)])  10.9 us
    all_to_all x1, starting transfers between devices, whole_body(): lax.all_to_all(jnp.broadcast_to(carry[None], (experts, *carry.shape)), 'e...  9.38 us
    pallas_call x1, Pallas kernels, mixer_local(): pl.pallas_call(mixer_kernel, out_shape=(full, full, full, jax.ShapeDtypeS...  8.53 us
    all_to_all x1, starting transfers between devices, whole_body(): lax.all_to_all(outgoing.reshape(experts, capacity, half), 'ep', 0, 0, til...  8.46 us
  transfers between devices with their start and end apart: 23, of which 9 were waited for; matrix products, arithmetic and copies ran while one was open for 5% of the time, Pallas kernels for 9%

profile of v1, /device:TPU:1, one launch (start us, length us, event | category | flops | bytes accessed | tf_op | source)
XLA Modules:
  0.0 193.3 jit_solution(4706261158762556422)
XLA Ops:
  0.7 1.7 copy-done.7
  2.4 1.6 copy-done.8
  4.0 0.7 copy-done.28
  4.7 0.7 copy-done.31
  5.4 5.3 %expert_front.1 = (bf16[768,2048]{1,0:T(8,128)(2,1)S(1)}, bf16[256,4096]{1,0:T(8,128)(2,1)S(1)}, s32[2,256]{1,0:T(2,128)S(1)}, bf16[8,4096]{1,0:T(8,128)(2,1)S(1)}) custom-call(s32[3]{0:T(128)S(1)} %pad_add_fusion.core.where.first, bf16[256,4096]{1,0:T(8,128)(2,1)S(1)} %copy-done.7, f32[1,4096]{1,0:T(1,128)S(1)} %bitcast.49, s32[2,256]{1,0:T(2,128)S(1)} %bitcast.51, ...), custom_call_target="tpu_custom_call" | custom-call | flops 5000000000 | bytes 5000000 | tf_op jit(solution)/shard_map/expert_front/pallas_call | solution.py:226
  10.7 1.7 copy-done.1
  12.4 8.5 %all-to-all-start = ((bf16[16,48,2048]{2,1,0:T(8,128)(2,1)}), bf16[16,48,2048]{2,1,0:T(8,128)(2,1)}, u32[]{:S(2)}, u32[]{:S(2)}) async-start(bf16[16,48,2048]{2,1,0:T(8,128)(2,1)} %bitcast.43), calls=%async_computation | async-start | bytes 6291456 | tf_op jit(solution)/shard_map/all_to_all | solution.py:468
  20.9 0.8 fusion.8
  22.1 0.7 fusion.refs_0_
  22.8 3.0 %collective-permute-start.3 = (bf16[256,128]{1,0:T(8,128)(2,1)S(1)}, bf16[256,128]{1,0:T(8,128)(2,1)S(1)}, u32[]{:S(2)}, u32[]{:S(2)}) collective-permute-start(bf16[256,128]{1,0:T(8,128)(2,1)S(1)} %fusion.refs_0_), channel_id=1, source_target_pairs={{0,4},{1,5},{2,6},{3,7},{4,0},{5,1},{6,2},{7,3},{8,12},{9,13},{10,... | collective-permute-start | bytes 196616 | tf_op jit(solution)/shard_map/ppermute | solution.py:439
  25.8 0.8 collective-permute-start.2
  26.6 0.7 collective-permute-start.1
  27.3 3.2 %collective-permute-start = (bf16[8,4096]{1,0:T(8,128)(2,1)S(1)}, bf16[8,4096]{1,0:T(8,128)(2,1)S(1)}, u32[]{:S(2)}, u32[]{:S(2)}) collective-permute-start(bf16[8,4096]{1,0:T(8,128)(2,1)S(1)} %get-tuple-element.33), channel_id=1, source_target_pairs={{0,8},{8,16},{16,24},{24,32},{32,40},{40,48},{48,56},{56,64},{64,7... | collective-permute-start | bytes 196616 | tf_op jit(solution)/shard_map/ppermute | solution.py:467
  30.7 0.9 prepared.1
  31.6 2.4 %collective-permute-start.7 = (bf16[2048,128]{1,0:T(8,128)(2,1)S(1)}, bf16[2048,128]{1,0:T(8,128)(2,1)S(1)}, u32[]{:S(2)}, u32[]{:S(2)}) collective-permute-start(bf16[2048,128]{1,0:T(8,128)(2,1)S(1)} %get-tuple-element.31), channel_id=1, source_target_pairs={{0,1},{1,0},{2,3},{3,2},{4,5},{5,4},{6,7},{7,6},{8,9},{9,8},{10,11... | collective-permute-start | bytes 1572872 | tf_op jit(solution)/shard_map/ppermute | solution.py:435
  34.0 28.7 %collective-permute-done.halo = bf16[8,4096]{1,0:T(8,128)(2,1)S(1)} collective-permute-done((bf16[8,4096]{1,0:T(8,128)(2,1)S(1)}, bf16[8,4096]{1,0:T(8,128)(2,1)S(1)}, u32[]{:S(2)}, u32[]{:S(2)}) %collective-permute-start) | collective-permute-done | bytes 65568 | tf_op jit(solution)/shard_map/ppermute | solution.py:467
  62.7 1.3 collective-permute-start.4
  63.9 1.5 collective-permute-start.5
  65.4 1.6 collective-permute-start.6
  67.1 2.4 %collective-permute-start.8 = (bf16[2048,128]{1,0:T(8,128)(2,1)S(1)}, bf16[2048,128]{1,0:T(8,128)(2,1)S(1)}, u32[]{:S(2)}, u32[]{:S(2)}) collective-permute-start(bf16[2048,128]{1,0:T(8,128)(2,1)S(1)} %get-tuple-element.45), channel_id=1, source_target_pairs={{0,1},{1,0},{2,3},{3,2},{4,5},{5,4},{6,7},{7,6},{8,9},{9,8},{10,11... | collective-permute-start | bytes 1572872 | tf_op jit(solution)/shard_map/ppermute | solution.py:435
  69.5 8.5 %mixer_local.1 = (f32[256,512]{1,0:T(8,128)S(1)}, f32[256,512]{1,0:T(8,128)S(1)}, f32[256,512]{1,0:T(8,128)S(1)}, f32[2,512]{1,0:T(2,128)S(1)}) custom-call(s32[3]{0:T(128)S(1)} %pad_add_fusion.core.where.first, bf16[256,4096]{1,0:T(8,128)(2,1)S(1)} %copy-done.9, bf16[8,4096]{1,0:T(8,128)(2,1)S(1)} %collective-permute-done.halo, f32[1,4096]{1,0:T(1,128)S(1)} %bitcast.50, ...), custom_call_target="tpu_custom_call" | custom-call | flops 8000000000 | bytes 8000000 | tf_op jit(solution)/shard_map/mixer_local/pallas_call | solution.py:141
  78.1 10.2 %collective-permute-done.6.refs_7_ = bf16[256,1024]{1,0:T(8,128)(2,1)S(1)} collective-permute-done((bf16[256,1024]{1,0:T(8,128)(2,1)S(1)}, bf16[256,1024]{1,0:T(8,128)(2,1)S(1)}, u32[]{:S(2)}, u32[]{:S(2)}) %collective-permute-start.6) | collective-permute-done | bytes 524320 | tf_op jit(solution)/shard_map/ppermute | solution.py:439
  88.3 1.8 down_parts.2
  90.2 0.8 copy-done.42
  91.0 0.8 copy-done.24
  91.8 0.8 copy-done.22
  92.6 1.0 copy-done.23
  93.7 1.0 copy-done.25
  94.7 3.8 %expert_parts.3 = f32[768,256]{1,0:T(8,128)S(1)} custom-call(s32[3]{0:T(128)S(1)} %pad_add_fusion.core.where.first, bf16[768,2048]{1,0:T(8,128)(2,1)} %bitcast.11.received_hbm, bf16[2048,128]{1,0:T(8,128)(2,1)S(1)} %copy-done.23, bf16[2048,128]{1,0:T(8,128)(2,1)S(1)} %copy-done.25), custom_call_target="tpu_custom_call" | custom-call | flops 3000000000 | bytes 3000000 | tf_op jit(solution)/shard_map/expert_parts/pallas_call | solution.py:280
  98.5 2.5 %collective-permute-start.9 = (f32[768,256]{1,0:T(8,128)S(1)}, f32[768,256]{1,0:T(8,128)S(1)}, u32[]{:S(2)}, u32[]{:S(2)}) collective-permute-start(f32[768,256]{1,0:T(8,128)S(1)} %expert_parts.3), channel_id=1, source_target_pairs={{0,1},{1,0},{2,3},{3,2},{4,5},{5,4},{6,7},{7,6},{8,9},{9,8},{10,11... | collective-permute-start | bytes 2359304 | tf_op jit(solution)/shard_map/ppermute | solution.py:435
  101.0 3.8 %expert_parts.2 = f32[768,256]{1,0:T(8,128)S(1)} custom-call(s32[3]{0:T(128)S(1)} %pad_add_fusion.core.where.first, bf16[768,2048]{1,0:T(8,128)(2,1)} %bitcast.11.received_hbm, bf16[4096,128]{1,0:T(8,128)(2,1)S(1)} %bitcast.46, bf16[4096,128]{1,0:T(8,128)(2,1)S(1)} %bitcast.48), custom_call_target="tpu_custom_call" | custom-call | flops 3000000000 | bytes 3000000 | tf_op jit(solution)/shard_map/expert_parts/pallas_call | solution.py:280
  105.1 0.6 collective-permute-start.12
  105.6 2.8 %collective-permute-start.11 = (bf16[768,128]{1,0:T(8,128)(2,1)S(1)}, bf16[768,128]{1,0:T(8,128)(2,1)S(1)}, u32[]{:S(2)}, u32[]{:S(2)}) collective-permute-start(bf16[768,128]{1,0:T(8,128)(2,1)S(1)} %fusion.4.refs_0_), channel_id=1, source_target_pairs={{0,6},{1,7},{2,0},{3,1},{4,2},{5,3},{6,4},{7,5},{8,14},{9,15},{10,... | collective-permute-start | bytes 589832 | tf_op jit(solution)/shard_map/ppermute | solution.py:439
  108.4 0.6 broadcast_in_dim.2
  109.1 9.4 %all-to-all-start.1 = ((f32[16,2,512]{2,1,0:T(2,128)}), f32[16,2,512]{2,1,0:T(2,128)S(1)}, u32[]{:S(2)}, u32[]{:S(2)}) async-start(f32[16,2,512]{2,1,0:T(2,128)} %broadcast_in_dim.2), calls=%async_computation.1 | async-start | bytes 131072 | tf_op jit(solution)/shard_map/all_to_all | solution.py:498
  118.5 1.0 copy-done.41
  119.5 2.1 %down_parts.3 = (f32[768,512]{1,0:T(8,128)S(1)}, f32[768,512]{1,0:T(8,128)S(1)}) custom-call(s32[3]{0:T(128)S(1)} %pad_add_fusion.core.where.first, bf16[768,128]{1,0:T(8,128)(2,1)S(1)} %fusion.4.refs_0_, bf16[768,128]{1,0:T(8,128)(2,1)} %collective-permute-done.10.refs_1_, bf16[768,128]{1,0:T(8,128)(2,1)S(1)} %collective-permute-done.11.refs_2_, ...), custom_call_target="tpu_custom_call" | custom-call | flops 2500000000 | bytes 2500000 | tf_op jit(solution)/shard_map/down_parts/pallas_call | solution.py:356
  121.6 1.2 copy-done.2
  122.8 1.2 copy-done.10
  124.0 1.0 all-to-all-done.1.carries
  125.0 2.2 %copy-done.6 = bf16[512,4096]{1,0:T(8,128)(2,1)S(1)} copy-done((bf16[512,4096]{1,0:T(8,128)(2,1)S(1)}, bf16[512,4096]{1,0:T(8,128)(2,1)}, u32[]{:S(2)}) %copy-start.6) | copy-done | bytes 4194328
  127.2 1.0 copy-done.35
  128.2 1.0 copy-done.37
  129.3 1.0 copy-done.39
  130.3 3.1 %mixer_out.1 = (f32[128,4096]{1,0:T(8,128)S(1)}, f32[128,4096]{1,0:T(8,128)}) custom-call(s32[3]{0:T(128)S(1)} %pad_add_fusion.core.where.first, f32[256,512]{1,0:T(8,128)S(1)} %copy-done.35, f32[256,512]{1,0:T(8,128)S(1)} %copy-done.37, f32[256,512]{1,0:T(8,128)S(1)} %copy-done.39, f32[16,2,512]{2,1,0:T(2,128)S(1)} %all-to-all-done.1.carries, ...), custom_call_target="tpu_custom_call" | custom-call | flops 3000000000 | bytes 3000000 | tf_op jit(solution)/shard_map/mixer_out/pallas_call | solution.py:393
  133.4 2.0 %collective-permute-start.13 = (f32[128,4096]{1,0:T(8,128)}, f32[128,4096]{1,0:T(8,128)}, u32[]{:S(2)}, u32[]{:S(2)}) collective-permute-start(f32[128,4096]{1,0:T(8,128)} %get-tuple-element.51), channel_id=1, source_target_pairs={{0,1},{1,0},{2,3},{3,2},{4,5},{5,4},{6,7},{7,6},{8,9},{9,8},{10,11... | collective-permute-start | bytes 6291464 | tf_op jit(solution)/shard_map/ppermute | solution.py:435
  135.6 6.1 %collective-permute-done.17 = f32[768,512]{1,0:T(8,128)S(1)} collective-permute-done((f32[768,512]{1,0:T(8,128)S(1)}, f32[768,512]{1,0:T(8,128)S(1)}, u32[]{:S(2)}, u32[]{:S(2)}) %collective-permute-start.17) | collective-permute-done | bytes 1572896 | tf_op jit(solution)/shard_map/ppermute | solution.py:435
  141.7 1.5 add.97
  143.2 6.5 %all-to-all-start.2 = ((f32[16,48,512]{2,1,0:T(8,128)}), f32[16,48,512]{2,1,0:T(8,128)}, u32[]{:S(2)}, u32[]{:S(2)}) async-start(f32[16,48,512]{2,1,0:T(8,128)} %bitcast.57), calls=%async_computation.2 | async-start | bytes 3145728 | tf_op jit(solution)/shard_map/all_to_all | solution.py:501
  149.8 1.9 %add.82 = f32[128,4096]{1,0:T(8,128)S(1)} add(f32[128,4096]{1,0:T(8,128)S(1)} %get-tuple-element.50, f32[128,4096]{1,0:T(8,128)} %collective-permute-done.13) | non-fusion elementwise | flops 524288 | bytes 6291456 | tf_op jit(solution)/shard_map/add | solution.py:507
  151.8 0.8 fusion.5
  152.6 0.5 collective-permute-start.14
  153.1 2.3 %collective-permute-start.16 = (bf16[32,4096]{1,0:T(8,128)(2,1)S(1)}, bf16[32,4096]{1,0:T(8,128)(2,1)S(1)}, u32[]{:S(2)}, u32[]{:S(2)}) collective-permute-start(bf16[32,4096]{1,0:T(8,128)(2,1)S(1)} %get-tuple-element.55), channel_id=1, source_target_pairs={{0,4},{1,5},{2,6},{3,7},{4,0},{5,1},{6,2},{7,3},{8,12},{9,13},{10,... | collective-permute-start | bytes 786440 | tf_op jit(solution)/shard_map/ppermute | solution.py:439
  155.3 0.7 collective-permute-start.15
  156.1 1.5 collective-permute-start.18
  157.6 3.8 %collective-permute-done.14 = bf16[32,4096]{1,0:T(8,128)(2,1)S(1)} collective-permute-done((bf16[32,4096]{1,0:T(8,128)(2,1)}, bf16[32,4096]{1,0:T(8,128)(2,1)S(1)}, u32[]{:S(2)}, u32[]{:S(2)}) %collective-permute-start.14) | collective-permute-done | bytes 262176 | tf_op jit(solution)/shard_map/ppermute | solution.py:439
  161.3 5.7 %collective-permute-done.16 = bf16[32,4096]{1,0:T(8,128)(2,1)S(1)} collective-permute-done((bf16[32,4096]{1,0:T(8,128)(2,1)S(1)}, bf16[32,4096]{1,0:T(8,128)(2,1)S(1)}, u32[]{:S(2)}, u32[]{:S(2)}) %collective-permute-start.16) | collective-permute-done | bytes 262176 | tf_op jit(solution)/shard_map/ppermute | solution.py:439
  167.2 1.3 multiply_reduce_fusion
  168.5 5.2 %all-to-all-done.2 = f32[16,48,512]{2,1,0:T(8,128)} async-done(((f32[16,48,512]{2,1,0:T(8,128)}), f32[16,48,512]{2,1,0:T(8,128)}, u32[]{:S(2)}, u32[]{:S(2)}) %all-to-all-start.2) | async-done | bytes 1572896 | tf_op jit(solution)/shard_map/all_to_all | solution.py:501
  173.8 3.8 %combine.1 = f32[256,512]{1,0:T(8,128)} custom-call(f32[768,512]{1,0:T(8,128)} %bitcast.18.back, s32[2,256]{1,0:T(2,128)S(1)} %get-tuple-element.29.slots, f32[2,256]{1,0:T(2,128)S(1)} %bitcast.53, f32[256,512]{1,0:T(8,128)S(1)} %copy-done.43, f32[256,512]{1,0:T(8,128)S(1)} %collective-permute-done.18.other), custom_call_target="tpu_custom_call" | custom-call | flops 3000000000 | bytes 3000000 | tf_op jit(solution)/shard_map/combine/pallas_call | solution.py:420
  177.6 5.3 %all-to-all-start.3 = ((f32[8,32,512]{2,1,0:T(8,128)}), f32[8,32,512]{2,1,0:T(8,128)S(1)}, u32[]{:S(2)}, u32[]{:S(2)}) async-start(f32[8,32,512]{2,1,0:T(8,128)} %bitcast.20), calls=%async_computation.3 | async-start | bytes 1048576 | tf_op jit(solution)/shard_map/all_to_all | solution.py:516
  182.9 1.9 multiply_convert_fusion.1
  184.8 7.5 %all-to-all-done.3 = f32[8,32,512]{2,1,0:T(8,128)S(1)} async-done(((f32[8,32,512]{2,1,0:T(8,128)}), f32[8,32,512]{2,1,0:T(8,128)S(1)}, u32[]{:S(2)}, u32[]{:S(2)}) %all-to-all-start.3) | async-done | bytes 524320 | tf_op jit(solution)/shard_map/all_to_all | solution.py:516
  192.5 0.8 multiply_convert_fusion
  (103 shorter events, 1.5 us)
Async XLA Ops:
  0.6 20.3 %copy-start = (bf16[4096,128]{1,0:T(8,128)(2,1)S(1)}, bf16[4096,128]{1,0:T(8,128)(2,1)}, u32[]{:S(2)}) copy-start(bf16[4096,128]{1,0:T(8,128)(2,1)} %param.38) | copy-start | bytes 3145732
  0.7 1.7 copy-start.7
  2.4 1.6 copy-start.8
  10.7 1.7 copy-start.1
  12.4 80.2 %all-to-all-start = ((bf16[16,48,2048]{2,1,0:T(8,128)(2,1)}), bf16[16,48,2048]{2,1,0:T(8,128)(2,1)}, u32[]{:S(2)}, u32[]{:S(2)}) async-start(bf16[16,48,2048]{2,1,0:T(8,128)(2,1)} %bitcast.43), calls=%async_computation | async-start | bytes 6291456 | tf_op jit(solution)/shard_map/all_to_all | solution.py:468
  20.9 1.2 copy-start.47
  20.9 9.6 %copy-start.16 = (bf16[1,4096,128]{2,1,0:T(8,128)(2,1)S(1)}, bf16[1,4096,128]{2,1,0:T(8,128)(2,1)}, u32[]{:S(2)}) copy-start(bf16[1,4096,128]{2,1,0:T(8,128)(2,1)} %param.36) | copy-start | bytes 3145732
  22.1 8.4 %copy-start.12 = (bf16[1,128,4096]{2,1,0:T(8,128)(2,1)S(1)}, bf16[1,128,4096]{2,1,0:T(8,128)(2,1)}, u32[]{:S(2)}) copy-start(bf16[1,128,4096]{2,1,0:T(8,128)(2,1)} %param.37) | copy-start | bytes 3145732
  22.1 8.4 %copy-start.13 = (bf16[128,4096]{1,0:T(8,128)(2,1)S(1)}, bf16[128,4096]{1,0:T(8,128)(2,1)}, u32[]{:S(2)}) copy-start(bf16[128,4096]{1,0:T(8,128)(2,1)} %shared.1) | copy-start | bytes 3145732
  22.1 8.4 %copy-start.14 = (bf16[1,4096,128]{2,1,0:T(8,128)(2,1)S(1)}, bf16[1,4096,128]{2,1,0:T(8,128)(2,1)}, u32[]{:S(2)}) copy-start(bf16[1,4096,128]{2,1,0:T(8,128)(2,1)} %param.35) | copy-start | bytes 3145732
  22.8 41.1 %collective-permute-start.3 = (bf16[256,128]{1,0:T(8,128)(2,1)S(1)}, bf16[256,128]{1,0:T(8,128)(2,1)S(1)}, u32[]{:S(2)}, u32[]{:S(2)}) collective-permute-start(bf16[256,128]{1,0:T(8,128)(2,1)S(1)} %fusion.refs_0_), channel_id=1, source_target_pairs={{0,4},{1,5},{2,6},{3,7},{4,0},{5,1},{6,2},{7,3},{8,12},{9,13},{10,... | collective-permute-start | bytes 196616 | tf_op jit(solution)/shard_map/ppermute | solution.py:439
  25.8 39.6 %collective-permute-start.2 = (bf16[256,128]{1,0:T(8,128)(2,1)S(1)}, bf16[256,128]{1,0:T(8,128)(2,1)S(1)}, u32[]{:S(2)}, u32[]{:S(2)}) collective-permute-start(bf16[256,128]{1,0:T(8,128)(2,1)S(1)} %fusion.refs_0_), channel_id=1, source_target_pairs={{0,6},{1,7},{2,0},{3,1},{4,2},{5,3},{6,4},{7,5},{8,14},{9,15},{10,... | collective-permute-start | bytes 196616 | tf_op jit(solution)/shard_map/ppermute | solution.py:439
  26.6 40.5 %collective-permute-start.1 = (bf16[256,128]{1,0:T(8,128)(2,1)S(1)}, bf16[256,128]{1,0:T(8,128)(2,1)S(1)}, u32[]{:S(2)}, u32[]{:S(2)}) collective-permute-start(bf16[256,128]{1,0:T(8,128)(2,1)S(1)} %fusion.refs_0_), channel_id=1, source_target_pairs={{0,2},{1,3},{2,4},{3,5},{4,6},{5,7},{6,0},{7,1},{8,10},{9,11},{10,... | collective-permute-start | bytes 196616 | tf_op jit(solution)/shard_map/ppermute | solution.py:439
  27.3 35.4 %collective-permute-start = (bf16[8,4096]{1,0:T(8,128)(2,1)S(1)}, bf16[8,4096]{1,0:T(8,128)(2,1)S(1)}, u32[]{:S(2)}, u32[]{:S(2)}) collective-permute-start(bf16[8,4096]{1,0:T(8,128)(2,1)S(1)} %get-tuple-element.33), channel_id=1, source_target_pairs={{0,8},{8,16},{16,24},{24,32},{32,40},{40,48},{48,56},{56,64},{64,7... | collective-permute-start | bytes 196616 | tf_op jit(solution)/shard_map/ppermute | solution.py:467
  30.6 38.9 %copy-start.4 = (bf16[4096,512]{1,0:T(8,128)(2,1)S(1)}, bf16[4096,512]{1,0:T(8,128)(2,1)}, u32[]{:S(2)}) copy-start(bf16[4096,512]{1,0:T(8,128)(2,1)} %gate_hbm.1) | copy-start | bytes 12582916
  30.6 38.9 %copy-start.5 = (bf16[4096,512]{1,0:T(8,128)(2,1)S(1)}, bf16[4096,512]{1,0:T(8,128)(2,1)}, u32[]{:S(2)}) copy-start(bf16[4096,512]{1,0:T(8,128)(2,1)} %input_hbm.1) | copy-start | bytes 12582916
  30.6 38.8 %copy-start.9 = (bf16[256,4096]{1,0:T(8,128)(2,1)S(1)}, bf16[256,4096]{1,0:T(8,128)(2,1)}, u32[]{:S(2)}) copy-start(bf16[256,4096]{1,0:T(8,128)(2,1)} %rows_hbm.3) | copy-start | bytes 6291460
  30.6 38.8 %copy-start.26 = (bf16[2,256,256]{2,1,0:T(8,128)(2,1)S(1)}, bf16[2,256,256]{2,1,0:T(8,128)(2,1)}, u32[]{:S(2)}) copy-start(bf16[2,256,256]{2,1,0:T(8,128)(2,1)} %in_gates.1) | copy-start | bytes 786436
  30.6 38.8 %copy-start.27 = (bf16[2,256,256]{2,1,0:T(8,128)(2,1)S(1)}, bf16[2,256,256]{2,1,0:T(8,128)(2,1)}, u32[]{:S(2)}) copy-start(bf16[2,256,256]{2,1,0:T(8,128)(2,1)} %de_gates.1) | copy-start | bytes 786436
  30.6 38.8 %copy-start.29 = (f32[4096]{0:T(1024)S(1)}, f32[4096]{0:T(1024)}, u32[]{:S(2)}) copy-start(f32[4096]{0:T(1024)} %param.22) | copy-start | bytes 49156
  30.6 38.8 %copy-start.30 = (f32[4,512]{1,0:T(4,128)S(1)}, f32[4,512]{1,0:T(4,128)}, u32[]{:S(2)}) copy-start(f32[4,512]{1,0:T(4,128)} %taps.1) | copy-start | bytes 24580
  30.7 38.8 %copy-start.32 = (f32[512]{0:T(512)S(1)}, f32[512]{0:T(512)}, u32[]{:S(2)}) copy-start(f32[512]{0:T(512)} %param.28) | copy-start | bytes 6148
  31.6 56.8 %copy-start.40 = (bf16[256,1024]{1,0:T(8,128)(2,1)}, bf16[256,1024]{1,0:T(8,128)(2,1)S(1)}, u32[]{:S(2)}) copy-start(bf16[256,1024]{1,0:T(8,128)(2,1)S(1)} %get-tuple-element.40.refs_4_) | copy-start | bytes 1572868
  31.6 60.2 %collective-permute-start.7 = (bf16[2048,128]{1,0:T(8,128)(2,1)S(1)}, bf16[2048,128]{1,0:T(8,128)(2,1)S(1)}, u32[]{:S(2)}, u32[]{:S(2)}) collective-permute-start(bf16[2048,128]{1,0:T(8,128)(2,1)S(1)} %get-tuple-element.31), channel_id=1, source_target_pairs={{0,1},{1,0},{2,3},{3,2},{4,5},{5,4},{6,7},{7,6},{8,9},{9,8},{10,11... | collective-permute-start | bytes 1572872 | tf_op jit(solution)/shard_map/ppermute | solution.py:435
  62.7 15.4 %collective-permute-start.4 = (bf16[256,1024]{1,0:T(8,128)(2,1)S(1)}, bf16[256,1024]{1,0:T(8,128)(2,1)S(1)}, u32[]{:S(2)}, u32[]{:S(2)}) collective-permute-start(bf16[256,1024]{1,0:T(8,128)(2,1)S(1)} %get-tuple-element.41), channel_id=1, source_target_pairs={{0,2},{1,3},{2,4},{3,5},{4,6},{5,7},{6,0},{7,1},{8,10},{9,11},{10,... | collective-permute-start | bytes 1572872 | tf_op jit(solution)/shard_map/ppermute | solution.py:439
  63.9 14.1 %collective-permute-start.5 = (bf16[256,1024]{1,0:T(8,128)(2,1)S(1)}, bf16[256,1024]{1,0:T(8,128)(2,1)S(1)}, u32[]{:S(2)}, u32[]{:S(2)}) collective-permute-start(bf16[256,1024]{1,0:T(8,128)(2,1)S(1)} %get-tuple-element.42), channel_id=1, source_target_pairs={{0,6},{1,7},{2,0},{3,1},{4,2},{5,3},{6,4},{7,5},{8,14},{9,15},{10,... | collective-permute-start | bytes 1572872 | tf_op jit(solution)/shard_map/ppermute | solution.py:439
  65.4 22.9 %collective-permute-start.6 = (bf16[256,1024]{1,0:T(8,128)(2,1)S(1)}, bf16[256,1024]{1,0:T(8,128)(2,1)S(1)}, u32[]{:S(2)}, u32[]{:S(2)}) collective-permute-start(bf16[256,1024]{1,0:T(8,128)(2,1)S(1)} %get-tuple-element.43), channel_id=1, source_target_pairs={{0,4},{1,5},{2,6},{3,7},{4,0},{5,1},{6,2},{7,3},{8,12},{9,13},{10,... | collective-permute-start | bytes 1572872 | tf_op jit(solution)/shard_map/ppermute | solution.py:439
  67.1 23.9 %collective-permute-start.8 = (bf16[2048,128]{1,0:T(8,128)(2,1)S(1)}, bf16[2048,128]{1,0:T(8,128)(2,1)S(1)}, u32[]{:S(2)}, u32[]{:S(2)}) collective-permute-start(bf16[2048,128]{1,0:T(8,128)(2,1)S(1)} %get-tuple-element.45), channel_id=1, source_target_pairs={{0,1},{1,0},{2,3},{3,2},{4,5},{5,4},{6,7},{7,6},{8,9},{9,8},{10,11... | collective-permute-start | bytes 1572872 | tf_op jit(solution)/shard_map/ppermute | solution.py:435
  78.0 12.1 %copy-start.34 = (f32[256,512]{1,0:T(8,128)}, f32[256,512]{1,0:T(8,128)S(1)}, u32[]{:S(2)}) copy-start(f32[256,512]{1,0:T(8,128)S(1)} %get-tuple-element.34.gate) | copy-start | bytes 1572868
  78.0 12.1 %copy-start.36 = (f32[256,512]{1,0:T(8,128)}, f32[256,512]{1,0:T(8,128)S(1)}, u32[]{:S(2)}) copy-start(f32[256,512]{1,0:T(8,128)S(1)} %get-tuple-element.35.states) | copy-start | bytes 1572868
  78.0 12.1 %copy-start.38 = (f32[256,512]{1,0:T(8,128)}, f32[256,512]{1,0:T(8,128)S(1)}, u32[]{:S(2)}) copy-start(f32[256,512]{1,0:T(8,128)S(1)} %get-tuple-element.36.decays) | copy-start | bytes 1572868
  78.1 12.1 %copy-start.18 = (bf16[256,1024]{1,0:T(8,128)(2,1)}, bf16[256,1024]{1,0:T(8,128)(2,1)S(1)}, u32[]{:S(2)}) copy-start(bf16[256,1024]{1,0:T(8,128)(2,1)S(1)} %collective-permute-done.5.refs_6_) | copy-start | bytes 1572868
  88.3 1.9 copy-start.20
  92.6 1.0 copy-start.23
  93.7 1.0 copy-start.25
  94.7 6.3 %copy-start.15 = (bf16[1,4096,128]{2,1,0:T(8,128)(2,1)S(1)}, bf16[1,4096,128]{2,1,0:T(8,128)(2,1)}, u32[]{:S(2)}) copy-start(bf16[1,4096,128]{2,1,0:T(8,128)(2,1)} %param.35) | copy-start | bytes 3145732
  94.7 6.3 %copy-start.17 = (bf16[1,4096,128]{2,1,0:T(8,128)(2,1)S(1)}, bf16[1,4096,128]{2,1,0:T(8,128)(2,1)}, u32[]{:S(2)}) copy-start(bf16[1,4096,128]{2,1,0:T(8,128)(2,1)} %param.36) | copy-start | bytes 3145732
  98.5 6.3 %collective-permute-start.9 = (f32[768,256]{1,0:T(8,128)S(1)}, f32[768,256]{1,0:T(8,128)S(1)}, u32[]{:S(2)}, u32[]{:S(2)}) collective-permute-start(f32[768,256]{1,0:T(8,128)S(1)} %expert_parts.3), channel_id=1, source_target_pairs={{0,1},{1,0},{2,3},{3,2},{4,5},{5,4},{6,7},{7,6},{8,9},{9,8},{10,11... | collective-permute-start | bytes 2359304 | tf_op jit(solution)/shard_map/ppermute | solution.py:435
  104.8 13.7 %copy-start.19 = (bf16[256,1024]{1,0:T(8,128)(2,1)S(1)}, bf16[256,1024]{1,0:T(8,128)(2,1)}, u32[]{:S(2)}) copy-start(bf16[256,1024]{1,0:T(8,128)(2,1)} %copy-done.18) | copy-start | bytes 1572868
  104.8 13.7 %copy-start.21 = (bf16[256,1024]{1,0:T(8,128)(2,1)S(1)}, bf16[256,1024]{1,0:T(8,128)(2,1)}, u32[]{:S(2)}) copy-start(bf16[256,1024]{1,0:T(8,128)(2,1)} %copy-done.20) | copy-start | bytes 1572868
  105.1 13.4 %collective-permute-start.12 = (bf16[768,128]{1,0:T(8,128)(2,1)S(1)}, bf16[768,128]{1,0:T(8,128)(2,1)S(1)}, u32[]{:S(2)}, u32[]{:S(2)}) collective-permute-start(bf16[768,128]{1,0:T(8,128)(2,1)S(1)} %fusion.4.refs_0_), channel_id=1, source_target_pairs={{0,4},{1,5},{2,6},{3,7},{4,0},{5,1},{6,2},{7,3},{8,12},{9,13},{10,... | collective-permute-start | bytes 589832 | tf_op jit(solution)/shard_map/ppermute | solution.py:439
  105.6 12.8 %collective-permute-start.11 = (bf16[768,128]{1,0:T(8,128)(2,1)S(1)}, bf16[768,128]{1,0:T(8,128)(2,1)S(1)}, u32[]{:S(2)}, u32[]{:S(2)}) collective-permute-start(bf16[768,128]{1,0:T(8,128)(2,1)S(1)} %fusion.4.refs_0_), channel_id=1, source_target_pairs={{0,6},{1,7},{2,0},{3,1},{4,2},{5,3},{6,4},{7,5},{8,14},{9,15},{10,... | collective-permute-start | bytes 589832 | tf_op jit(solution)/shard_map/ppermute | solution.py:439
  108.4 10.1 %collective-permute-start.10 = (bf16[768,128]{1,0:T(8,128)(2,1)S(1)}, bf16[768,128]{1,0:T(8,128)(2,1)}, u32[]{:S(2)}, u32[]{:S(2)}) collective-permute-start(bf16[768,128]{1,0:T(8,128)(2,1)S(1)} %fusion.4.refs_0_), channel_id=1, source_target_pairs={{0,2},{1,3},{2,4},{3,5},{4,6},{5,7},{6,0},{7,1},{8,10},{9,11},{10,... | collective-permute-start | bytes 589832 | tf_op jit(solution)/shard_map/ppermute | solution.py:439
  109.1 16.0 %all-to-all-start.1 = ((f32[16,2,512]{2,1,0:T(2,128)}), f32[16,2,512]{2,1,0:T(2,128)S(1)}, u32[]{:S(2)}, u32[]{:S(2)}) async-start(f32[16,2,512]{2,1,0:T(2,128)} %broadcast_in_dim.2), calls=%async_computation.1 | async-start | bytes 131072 | tf_op jit(solution)/shard_map/all_to_all | solution.py:498
  118.5 1.0 copy-start.41
  121.6 1.2 copy-start.2
  122.8 1.2 copy-start.10
  125.0 2.2 %copy-start.6 = (bf16[512,4096]{1,0:T(8,128)(2,1)S(1)}, bf16[512,4096]{1,0:T(8,128)(2,1)}, u32[]{:S(2)}) copy-start(bf16[512,4096]{1,0:T(8,128)(2,1)} %out_hbm.1) | copy-start | bytes 12582916
  127.2 1.0 copy-start.35
  130.3 5.1 %copy-start.11 = (f32[768,512]{1,0:T(8,128)S(1)}, f32[768,512]{1,0:T(8,128)}, u32[]{:S(2)}) copy-start(f32[768,512]{1,0:T(8,128)} %copy-done.10) | copy-start | bytes 4718596
  130.3 11.4 %copy-start.3 = (f32[768,512]{1,0:T(8,128)S(1)}, f32[768,512]{1,0:T(8,128)}, u32[]{:S(2)}) copy-start(f32[768,512]{1,0:T(8,128)} %copy-done.2) | copy-start | bytes 4718596
  133.4 16.4 %collective-permute-start.13 = (f32[128,4096]{1,0:T(8,128)}, f32[128,4096]{1,0:T(8,128)}, u32[]{:S(2)}, u32[]{:S(2)}) collective-permute-start(f32[128,4096]{1,0:T(8,128)} %get-tuple-element.51), channel_id=1, source_target_pairs={{0,1},{1,0},{2,3},{3,2},{4,5},{5,4},{6,7},{7,6},{8,9},{9,8},{10,11... | collective-permute-start | bytes 6291464 | tf_op jit(solution)/shard_map/ppermute | solution.py:435
  135.5 6.2 %collective-permute-start.17 = (f32[768,512]{1,0:T(8,128)S(1)}, f32[768,512]{1,0:T(8,128)S(1)}, u32[]{:S(2)}, u32[]{:S(2)}) collective-permute-start(f32[768,512]{1,0:T(8,128)S(1)} %copy-done.11), channel_id=1, source_target_pairs={{0,1},{1,0},{2,3},{3,2},{4,5},{5,4},{6,7},{7,6},{8,9},{9,8},{10,11... | collective-permute-start | bytes 4718600 | tf_op jit(solution)/shard_map/ppermute | solution.py:435
  143.2 30.6 %all-to-all-start.2 = ((f32[16,48,512]{2,1,0:T(8,128)}), f32[16,48,512]{2,1,0:T(8,128)}, u32[]{:S(2)}, u32[]{:S(2)}) async-start(f32[16,48,512]{2,1,0:T(8,128)} %bitcast.57), calls=%async_computation.2 | async-start | bytes 3145728 | tf_op jit(solution)/shard_map/all_to_all | solution.py:501
  151.8 4.3 %copy-start.44 = (f32[128,4096]{1,0:T(8,128)}, f32[128,4096]{1,0:T(8,128)S(1)}, u32[]{:S(2)}) copy-start(f32[128,4096]{1,0:T(8,128)S(1)} %add.82) | copy-start | bytes 6291460
  151.8 22.0 %copy-start.33 = (f32[256,2]{0,1:T(2,128)S(1)}, f32[256,2]{0,1:T(2,128)}, u32[]{:S(2)}) copy-start(f32[256,2]{0,1:T(2,128)} %param.34) | copy-start | bytes 6148
  151.8 22.0 %copy-start.43 = (f32[256,512]{1,0:T(8,128)S(1)}, f32[256,512]{1,0:T(8,128)}, u32[]{:S(2)}) copy-start(f32[256,512]{1,0:T(8,128)} %copy-done.42) | copy-start | bytes 1572868
  152.6 8.7 %collective-permute-start.14 = (bf16[32,4096]{1,0:T(8,128)(2,1)}, bf16[32,4096]{1,0:T(8,128)(2,1)S(1)}, u32[]{:S(2)}, u32[]{:S(2)}) collective-permute-start(bf16[32,4096]{1,0:T(8,128)(2,1)} %get-tuple-element.54), channel_id=1, source_target_pairs={{0,2},{1,3},{2,4},{3,5},{4,6},{5,7},{6,0},{7,1},{8,10},{9,11},{10,... | collective-permute-start | bytes 786440 | tf_op jit(solution)/shard_map/ppermute | solution.py:439
  153.1 13.9 %collective-permute-start.16 = (bf16[32,4096]{1,0:T(8,128)(2,1)S(1)}, bf16[32,4096]{1,0:T(8,128)(2,1)S(1)}, u32[]{:S(2)}, u32[]{:S(2)}) collective-permute-start(bf16[32,4096]{1,0:T(8,128)(2,1)S(1)} %get-tuple-element.55), channel_id=1, source_target_pairs={{0,4},{1,5},{2,6},{3,7},{4,0},{5,1},{6,2},{7,3},{8,12},{9,13},{10,... | collective-permute-start | bytes 786440 | tf_op jit(solution)/shard_map/ppermute | solution.py:439
  155.3 11.9 %collective-permute-start.15 = (bf16[32,4096]{1,0:T(8,128)(2,1)S(1)}, bf16[32,4096]{1,0:T(8,128)(2,1)S(1)}, u32[]{:S(2)}, u32[]{:S(2)}) collective-permute-start(bf16[32,4096]{1,0:T(8,128)(2,1)S(1)} %get-tuple-element.56), channel_id=1, source_target_pairs={{0,6},{1,7},{2,0},{3,1},{4,2},{5,3},{6,4},{7,5},{8,14},{9,15},{10,... | collective-permute-start | bytes 786440 | tf_op jit(solution)/shard_map/ppermute | solution.py:439
  156.1 12.5 %collective-permute-start.18 = (f32[256,512]{1,0:T(8,128)}, f32[256,512]{1,0:T(8,128)S(1)}, u32[]{:S(2)}, u32[]{:S(2)}) collective-permute-start(f32[256,512]{1,0:T(8,128)} %get-tuple-element.53), channel_id=1, source_target_pairs={{0,1},{1,0},{2,3},{3,2},{4,5},{5,4},{6,7},{7,6},{8,9},{9,8},{10,11... | collective-permute-start | bytes 1572872 | tf_op jit(solution)/shard_map/ppermute | solution.py:435
  173.8 9.1 %copy-start.45 = (f32[4096]{0:T(1024)S(1)}, f32[4096]{0:T(1024)}, u32[]{:S(2)}) copy-start(f32[4096]{0:T(1024)} %param.30) | copy-start | bytes 49156
  177.6 14.9 %copy-start.46 = (f32[4096]{0:T(1024)S(1)}, f32[4096]{0:T(1024)}, u32[]{:S(2)}) copy-start(f32[4096]{0:T(1024)} %param.41) | copy-start | bytes 49156
  177.6 14.7 %all-to-all-start.3 = ((f32[8,32,512]{2,1,0:T(8,128)}), f32[8,32,512]{2,1,0:T(8,128)S(1)}, u32[]{:S(2)}, u32[]{:S(2)}) async-start(f32[8,32,512]{2,1,0:T(8,128)} %bitcast.20), calls=%async_computation.3 | async-start | bytes 1048576 | tf_op jit(solution)/shard_map/all_to_all | solution.py:516
  (7 other events, 5.9 us)

commit v2 on v1

--- a/solution.py
+++ b/solution.py
@@ -18,12 +18,13 @@
     return pl.BlockSpec(memory_space=pltpu.VMEM)
 
 
-def smem():
-    return pl.BlockSpec(memory_space=pltpu.SMEM)
+def seat():
+    tp = lax.axis_index("tp")
+    return tp % 2, tp // 2, lax.axis_index("ep")
 
 
 def hbm():
-    return pl.BlockSpec(memory_space=pltpu.HBM)
+    return pl.BlockSpec(memory_space=pl.ANY)
 
 
 def params(mib, micros):
@@ -59,7 +60,7 @@
 
 
 def mixer_kernel(
-    first, rows_hbm, halo, gain, gate_hbm, input_hbm, taps, in_gates, de_gates, offset,
+    rows_hbm, halo, gain, gate_hbm, input_hbm, taps, in_gates, de_gates, offset,
     gate_out, states_out, decay_out, carry_out, rows, normed, weights, sems,
 ):
     count = rows.shape[0]
@@ -114,7 +115,7 @@
     log_decay = -lru_power * decay_gate * softplus
     row_ids = lax.broadcasted_iota(jnp.int32, log_decay.shape, 0)
     scale = jnp.sqrt(minus_expm1(2.0 * log_decay))
-    scale = jnp.where((row_ids == 0) & (first[2] == 0), 1.0, scale)
+    scale = jnp.where((row_ids == 0) & (seat()[2] == 0), 1.0, scale)
     state = scale * input_gate * conv.astype(f32)
     decay = jnp.exp(log_decay)
     step = 1
@@ -135,13 +136,13 @@
     )
 
 
-def mixer_local(first, rows, halo, gain, gate_proj, input_proj, taps, in_gates, de_gates, offset):
+def mixer_local(rows, halo, gain, gate_proj, input_proj, taps, in_gates, de_gates, offset):
     count, width = rows.shape[0], gate_proj.shape[1]
     full = jax.ShapeDtypeStruct((count, width), f32)
     return pl.pallas_call(
         mixer_kernel,
         out_shape=(full, full, full, jax.ShapeDtypeStruct((2, width), f32)),
-        in_specs=[smem(), hbm(), vmem(), vmem(), hbm(), hbm(), vmem(), vmem(), vmem(), vmem()],
+        in_specs=[hbm(), vmem(), vmem(), hbm(), hbm(), vmem(), vmem(), vmem(), vmem()],
         out_specs=(vmem(), vmem(), vmem(), vmem()),
         scratch_shapes=[
             pltpu.VMEM(rows.shape, bf16),
@@ -150,12 +151,12 @@
             pltpu.SemaphoreType.DMA((6,)),
         ],
         name="mixer_local",
-        **params(24, 8),
-    )(first, rows, halo, gain, gate_proj, input_proj, taps, in_gates, de_gates, offset)
+        **params(58, 8),
+    )(rows, halo, gain, gate_proj, input_proj, taps, in_gates, de_gates, offset)
 
 
 def front_kernel(
-    core, rows_hbm, gain, ids, mixer_hbm, out_hbm, normed_hbm, slots, tail,
+    rows_hbm, gain, ids, mixer_hbm, out_hbm, normed_hbm, slots, tail,
     rows, normed, out, sems, *, experts, capacity,
 ):
     count, _ = rows.shape
@@ -204,7 +205,7 @@
         )
         save.start()
         saves.append(save)
-    mine = normed[:, pl.ds(pl.multiple_of(core[0] * half, half), half)]
+    mine = normed[:, pl.ds(pl.multiple_of(seat()[0] * half, half), half)]
     blocks = 3
     size = experts * capacity // blocks
     for k in range(blocks):
@@ -221,7 +222,7 @@
         c.wait()
 
 
-def expert_front(core, rows, gain, ids, mixer_rows, experts, capacity):
+def expert_front(rows, gain, ids, mixer_rows, experts, capacity):
     count, width = rows.shape
     return pl.pallas_call(
         functools.partial(front_kernel, experts=experts, capacity=capacity),
@@ -231,7 +232,7 @@
             jax.ShapeDtypeStruct((2, count), jnp.int32),
             jax.ShapeDtypeStruct((8, width), bf16),
         ),
-        in_specs=[smem(), hbm(), vmem(), vmem(), hbm()],
+        in_specs=[hbm(), vmem(), vmem(), hbm()],
         out_specs=(hbm(), hbm(), vmem(), vmem()),
         scratch_shapes=[
             pltpu.VMEM((count, width), bf16),
@@ -240,26 +241,29 @@
             pltpu.SemaphoreType.DMA((12,)),
         ],
         name="expert_front",
-        **params(20, 5),
-    )(core, rows, gain, ids, mixer_rows)
-
-
-def parts_kernel(core, received_hbm, gate, up, out, received, weights, sems, *, whole):
-    half, width = weights.shape[0], gate.shape[1]
-    start = pl.multiple_of(core[0] * half, half) if whole else 0
-    copies = [
-        pltpu.make_async_copy(
-            src.at[pl.ds(start, half), :], weights.at[:, k * width : (k + 1) * width], sems.at[k]
-        )
-        for k, src in enumerate((gate, up))
-    ]
-    pieces = 3
+        **params(58, 5),
+    )(rows, gain, ids, mixer_rows)
+
+
+def parts_kernel(received_hbm, *refs):
+    sources, (keep, send, received, weights, sems) = refs[:4], refs[4:]
+    half, width = weights.shape[0], sources[0].shape[1]
+    start = pl.multiple_of(seat()[0] * half, half)
+    copies = []
+    for k, src in enumerate(sources):
+        rows = pl.ds(start, half) if src.shape[0] > half else pl.ds(0, half)
+        copies.append(
+            pltpu.make_async_copy(
+                src.at[rows, :], weights.at[:, k * width : (k + 1) * width], sems.at[k]
+            )
+        )
+    pieces = 4
     part = received.shape[0] // pieces
     loads = [
         pltpu.make_async_copy(
             received_hbm.at[k * part : (k + 1) * part, :],
             received.at[k * part : (k + 1) * part, :],
-            sems.at[2 + k],
+            sems.at[4 + k],
         )
         for k in range(pieces)
     ]
@@ -269,68 +273,90 @@
         c.wait()
     for k in range(pieces):
         loads[k].wait()
-        out[k * part : (k + 1) * part, :] = jnp.dot(
+        both = jnp.dot(
             received[k * part : (k + 1) * part, :], weights[...], preferred_element_type=f32
         )
-
-
-def expert_parts(core, received, gate, up, whole):
+        keep[k * part : (k + 1) * part, :] = both[:, : 2 * width]
+        send[k * part : (k + 1) * part, :] = both[:, 2 * width :]
+
+
+def expert_parts(received, *weights):
     rows, half = received.shape
-    width = gate.shape[1]
-    return pl.pallas_call(
-        functools.partial(parts_kernel, whole=whole),
-        out_shape=jax.ShapeDtypeStruct((rows, 2 * width), f32),
-        in_specs=[smem(), hbm(), hbm(), hbm()],
-        out_specs=vmem(),
+    width = weights[0].shape[1]
+    shape = jax.ShapeDtypeStruct((rows, 2 * width), f32)
+    return pl.pallas_call(
+        parts_kernel,
+        out_shape=(shape, shape),
+        in_specs=[hbm()] * 5,
+        out_specs=(vmem(), vmem()),
         scratch_shapes=[
             pltpu.VMEM(received.shape, bf16),
-            pltpu.VMEM((half, 2 * width), bf16),
-            pltpu.SemaphoreType.DMA((5,)),
+            pltpu.VMEM((half, 4 * width), bf16),
+            pltpu.SemaphoreType.DMA((8,)),
         ],
         name="expert_parts",
-        **params(8, 3),
-    )(core, received, gate, up)
-
-
-def prep_kernel(where, gate, up, down, shared, gate_out, up_out, *refs):
-    outs, sems = refs[:4], refs[4]
+        **params(12, 5),
+    )(received, *weights)
+
+
+def prep_kernel(gate, up, down, shared, gate_out, up_out, *refs):
+    outs, (tall, wide, sems) = refs[:4], refs[4:]
     half, quarter = gate_out.shape[0], outs[0].shape[1]
     size = down.shape[0]
-    start = pl.multiple_of((1 - where[0]) * half, half)
-    copies = [
-        pltpu.make_async_copy(src.at[pl.ds(start, half), :], dst, sems.at[k])
-        for k, (src, dst) in enumerate(((gate, gate_out), (up, up_out)))
-    ]
+    core, chip, _ = seat()
+    start = pl.multiple_of((1 - core) * half, half)
+    moves = [
+        ((src.at[pl.ds(start, half), :], tall.at[k]),) for k, src in enumerate((gate, up))
+    ]
+    targets = [(tall.at[0], gate_out), (tall.at[1], up_out)]
     for s in range(4):
-        cols = pl.ds(pl.multiple_of(((where[1] + s) % 4) * quarter, quarter), quarter)
-        for k, src in enumerate((down, shared)):
-            copies.append(
-                pltpu.make_async_copy(
-                    src.at[:, cols], outs[s].at[k * size : (k + 1) * size, :], sems.at[2 + 2 * s + k]
-                )
+        cols = pl.ds(pl.multiple_of(((chip + s) % 4) * quarter, quarter), quarter)
+        moves.append(
+            tuple(
+                (src.at[:, cols], wide.at[s, k * size : (k + 1) * size, :])
+                for k, src in enumerate((down, shared))
             )
-    for c in copies:
-        c.start()
-    for c in copies:
+        )
+        targets.append((wide.at[s], outs[s]))
+    loads, n = [], 0
+    for group in moves:
+        made = []
+        for src, dst in group:
+            made.append(pltpu.make_async_copy(src, dst, sems.at[n]))
+            made[-1].start()
+            n += 1
+        loads.append(made)
+    saves = []
+    for made, (src, dst) in zip(loads, targets):
+        for c in made:
+            c.wait()
+        saves.append(pltpu.make_async_copy(src, dst, sems.at[n]))
+        saves[-1].start()
+        n += 1
+    for c in saves:
         c.wait()
 
 
-def prepared(where, gate, up, down, shared):
+def prepared(gate, up, down, shared):
     half, width = gate.shape[0] // 2, gate.shape[1]
     tall = jax.ShapeDtypeStruct((half, width), bf16)
     wide = jax.ShapeDtypeStruct((2 * down.shape[0], down.shape[1] // 4), bf16)
     return pl.pallas_call(
         prep_kernel,
         out_shape=(tall, tall, wide, wide, wide, wide),
-        in_specs=[smem()] + [hbm()] * 4,
+        in_specs=[hbm()] * 4,
         out_specs=(hbm(),) * 6,
-        scratch_shapes=[pltpu.SemaphoreType.DMA((10,))],
+        scratch_shapes=[
+            pltpu.VMEM((2, *tall.shape), bf16),
+            pltpu.VMEM((4, *wide.shape), bf16),
+            pltpu.SemaphoreType.DMA((16,)),
+        ],
         name="prepared",
-        **params(2, 3),
-    )(where, gate, up, down, shared)
-
-
-def down_kernel(core, *refs, at):
+        **params(58, 3),
+    )(gate, up, down, shared)
+
+
+def down_kernel(*refs, at):
     hidden, weights, (keep, send, w, sems) = refs[:4], refs[4:8], refs[8:]
     size = hidden[0].shape[1]
     width = keep.shape[1]
@@ -345,18 +371,18 @@
     h = jnp.concatenate([p[...] for p in hidden], axis=1)
     for c in copies:
         c.wait()
-    for out, which in ((send, 1 - core[0]), (keep, core[0])):
+    for out, which in ((send, 1 - seat()[0]), (keep, seat()[0])):
         cols = pl.ds(pl.multiple_of(which * width, width), width)
         out[...] = jnp.dot(h, w[:, cols], preferred_element_type=f32)
 
 
-def down_parts(core, hidden, weights, at):
+def down_parts(hidden, weights, at):
     width = weights[0].shape[1] // 2
     shape = jax.ShapeDtypeStruct((hidden[0].shape[0], width), f32)
     return pl.pallas_call(
         functools.partial(down_kernel, at=at),
         out_shape=(shape, shape),
-        in_specs=[smem()] + [vmem()] * 4 + [hbm()] * 4,
+        in_specs=[vmem()] * 4 + [hbm()] * 4,
         out_specs=(vmem(), vmem()),
         scratch_shapes=[
             pltpu.VMEM((4 * hidden[0].shape[1], 2 * width), bf16),
@@ -364,56 +390,86 @@
         ],
         name="down_parts",
         **params(10, 2.5),
-    )(core, *hidden, *weights)
-
-
-def mixer_out_kernel(where, gate, states, decays, carries, out_hbm, keep, send, gated, weights, sem):
-    load = pltpu.make_async_copy(out_hbm, weights, sem)
-    load.start()
+    )(*hidden, *weights)
+
+
+def mixer_out_kernel(
+    gate_hbm, states_hbm, decays_hbm, carries, out_hbm, keep_hbm, send_hbm,
+    gate, states, decays, weights, gated, keep, send, sems,
+):
+    core, _, ep = seat()
+    loads = [
+        pltpu.make_async_copy(src, dst, sems.at[k])
+        for k, (src, dst) in enumerate(((gate_hbm, gate), (states_hbm, states), (decays_hbm, decays)))
+    ]
+    pieces = 4
+    part = keep.shape[1] // pieces
+    spans = [slice(k * part, (k + 1) * part) for k in range(pieces)]
+    for k, span in enumerate(spans):
+        loads.append(pltpu.make_async_copy(out_hbm.at[:, span], weights.at[:, span], sems.at[3 + k]))
+    for c in loads:
+        c.start()
     carried = jnp.zeros((1, gate.shape[1]), f32)
     for i in range(carries.shape[0] - 1):
-        carried = jnp.where(i < where[2], carries[i, 0:1] * carried + carries[i, 1:2], carried)
-    gated[...] = (gate[...] * (states[...] + decays[...] * carried)).astype(bf16)
+        carried = jnp.where(i < ep, carries[i, 0:1] * carried + carries[i, 1:2], carried)
+    for c in loads[:3]:
+        c.wait()
+    values = (gate[...] * (states[...] + decays[...] * carried)).astype(bf16)
     rows = keep.shape[0] // 4
-    load.wait()
-    for out, which in ((send, 1 - where[0]), (keep, where[0])):
-        picked = jnp.concatenate(
-            [
-                gated[pl.ds(pl.multiple_of((2 * i + which) * rows, rows), rows), :]
-                for i in range(4)
-            ],
-            axis=0,
-        )
-        out[...] = jnp.dot(picked, weights[...], preferred_element_type=f32)
-
-
-def mixer_out_parts(where, gate, states, decays, carries, out_proj):
+    for i in range(8):
+        target = pl.multiple_of(jnp.where(core == i % 2, 4 + i // 2, i // 2) * rows, rows)
+        gated[pl.ds(target, rows), :] = values[i * rows : (i + 1) * rows, :]
+    saves = []
+    for k, span in enumerate(spans):
+        loads[3 + k].wait()
+        both = jnp.dot(gated[...], weights[:, span], preferred_element_type=f32)
+        send[:, span] = both[: 4 * rows]
+        keep[:, span] = both[4 * rows :]
+        for j, (src, dst) in enumerate(((send, send_hbm), (keep, keep_hbm))):
+            saves.append(
+                pltpu.make_async_copy(src.at[:, span], dst.at[:, span], sems.at[7 + 2 * k + j])
+            )
+            saves[-1].start()
+    for c in saves:
+        c.wait()
+
+
+def mixer_out_parts(gate, states, decays, carries, out_proj):
     rows, width = gate.shape[0], out_proj.shape[1]
     shape = jax.ShapeDtypeStruct((rows // 2, width), f32)
     return pl.pallas_call(
         mixer_out_kernel,
         out_shape=(shape, shape),
-        in_specs=[smem()] + [vmem()] * 4 + [hbm()],
-        out_specs=(vmem(), vmem()),
-        scratch_shapes=[
+        in_specs=[hbm(), hbm(), hbm(), vmem(), hbm()],
+        out_specs=(hbm(), hbm()),
+        scratch_shapes=[pltpu.VMEM(gate.shape, f32)] * 3
+        + [
+            pltpu.VMEM(out_proj.shape, bf16),
             pltpu.VMEM(gate.shape, bf16),
-            pltpu.VMEM(out_proj.shape, bf16),
-            pltpu.SemaphoreType.DMA,
+            pltpu.VMEM(shape.shape, f32),
+            pltpu.VMEM(shape.shape, f32),
+            pltpu.SemaphoreType.DMA((15,)),
         ],
         name="mixer_out",
-        **params(16, 3),
-    )(where, gate, states, decays, carries, out_proj)
+        **params(58, 3),
+    )(gate, states, decays, carries, out_proj)
 
 
 def combine_kernel(back, slots, weights, own, other, out):
-    down = lax.broadcasted_iota(jnp.int32, (back.shape[0], slots.shape[1]), 0)
-    mix = jnp.where(slots[0:1, :] == down, weights[0:1, :], 0.0) + jnp.where(
-        slots[1:2, :] == down, weights[1:2, :], 0.0
-    )
-    out[...] = own[...] + other[...] + lax.dot_general(
-        mix, back[...], (((0,), (0,)), ((), ())), preferred_element_type=f32,
-        precision=lax.Precision.HIGHEST,
-    )
+    count = slots.shape[1]
+    down = lax.broadcasted_iota(jnp.int32, (back.shape[0], count), 0)
+    same = lax.broadcasted_iota(jnp.int32, (count, count), 0) == lax.broadcasted_iota(
+        jnp.int32, (count, count), 1
+    )
+    total = own[...] + other[...]
+    for k in range(2):
+        hit = jnp.where(slots[k : k + 1, :] == down, 1.0, 0.0).astype(bf16)
+        picked = lax.dot_general(
+            hit, back[...], (((0,), (0,)), ((), ())), preferred_element_type=f32
+        )
+        weight = jnp.sum(jnp.where(same, weights[k : k + 1, :], 0.0), axis=1, keepdims=True)
+        total = total + weight * picked
+    out[...] = total
 
 
 def combined(back, slots, weights, own, other):
@@ -452,9 +508,8 @@
     decay_offset, out_proj, mixer_scale, expert_rows, expert_gain, route_ids, route_weights,
     expert_gate, expert_up, expert_down, shared_gate, shared_up, shared_down, expert_scale,
 ):
-    ep_index, tp_index = lax.axis_index("ep"), lax.axis_index("tp")
-    core, chip = tp_index % 2, tp_index // 2
-    where = jnp.stack([core, chip, ep_index])
+    tp_index = lax.axis_index("tp")
+    chip = tp_index // 2
     rows, width = mixer_rows.shape
     experts = lax.axis_size("ep")
     capacity = rows * 2 * 3 // (2 * experts)
@@ -462,7 +517,7 @@
     order = (1, 3, 2)
 
     outgoing, expert_normed, slots, tail = expert_front(
-        where, expert_rows, expert_gain.reshape(1, -1), route_ids.T, mixer_rows, experts, capacity
+        expert_rows, expert_gain.reshape(1, -1), route_ids.T, mixer_rows, experts, capacity
     )
     halo = lax.ppermute(tail, "ep", [(i, i + 1) for i in range(15)])
     received = lax.all_to_all(
@@ -470,7 +525,7 @@
     ).reshape(experts * capacity, half)
 
     send_gate, send_up, *downs = prepared(
-        after(where, slots), expert_gate[0], expert_up[0], expert_down[0], shared_down
+        expert_gate[0], expert_up[0], after(expert_down[0], slots), shared_down
     )
     shared_hidden = (
         jax.nn.silu(jnp.dot(expert_normed, shared_gate, preferred_element_type=f32))
@@ -481,29 +536,35 @@
     downs = [downs[0]] + [turned(downs[s], s) for s in order]
 
     gate_branch, local_states, decay_product, carry = mixer_local(
-        after(where, shared_hidden, send_gate), mixer_rows, halo, mixer_gain.reshape(1, -1), gate_proj, input_proj,
+        after(mixer_rows, shared_hidden, send_gate), halo, mixer_gain.reshape(1, -1), gate_proj, input_proj,
         conv_taps, input_gates, decay_gates, decay_offset.reshape(1, -1),
     )
     hidden_width = expert_gate.shape[2]
-    shared_keep, shared_send = down_parts(after(where, carry), shared_all, downs, hidden_width)
-    shared_other = swapped(shared_send)
-
-    received = after(received, carry, shared_keep, other_gate, other_up)
-    other_part = expert_parts(where, received, other_gate, other_up, False)
-    own_part = expert_parts(where, received, expert_gate[0], expert_up[0], True)
+    received = after(received, carry)
+    own_part, other_part = expert_parts(
+        received, expert_gate[0], expert_up[0], other_gate, other_up
+    )
     parts = own_part + swapped(other_part)
     copy_hidden = (jax.nn.silu(parts[:, :hidden_width]) * parts[:, hidden_width:]).astype(bf16)
     hidden_all = gathered(copy_hidden)
     carry = after(carry, copy_hidden)
-    carries = lax.all_to_all(jnp.broadcast_to(carry[None], (experts, *carry.shape)), "ep", 0, 0, tiled=True)
-    keep_result, send_result = down_parts(where, hidden_all, downs, 0)
-    results = keep_result + swapped(send_result)
+    carries = lax.all_to_all(
+        jnp.broadcast_to(carry[None], (experts, *carry.shape)), "ep", 0, 0, tiled=True
+    )
+    keep_result, send_result = down_parts(hidden_all, downs, 0)
+    results = (keep_result + swapped(send_result)).astype(bf16)
+    shared_keep, shared_send = down_parts(
+        [after(shared_all[0], results), *shared_all[1:]], downs, hidden_width
+    )
+    shared_other = swapped(shared_send)
     back = lax.all_to_all(
         results.reshape(experts, capacity, -1), "ep", 0, 0, tiled=True
     ).reshape(experts * capacity, -1)
 
     carries = after(carries, keep_result)
-    keep_term, send_term = mixer_out_parts(where, gate_branch, local_states, decay_product, carries, out_proj)
+    keep_term, send_term = mixer_out_parts(
+        gate_branch, local_states, decay_product, carries, out_proj
+    )
     pair_term = (keep_term + swapped(send_term)).reshape(4, rows // 8, width)
     mixer_sum = lax.dynamic_index_in_dim(pair_term, chip, 0, keepdims=False)
     for s in order:

time: 194 us -> 180 us (0.928)
  waiting for transfers between devices: 68.4 us -> 56.3 us
  local copies, waits for them, and re-layouts: 21.6 us -> 16.8 us
  other arithmetic: 7.97 us -> 9.94 us
    ppermute x12, starting transfers between devices: 15.6 us -> 22.4 us  [turned(): return lax.ppermute(block, 'tp', [(i, (i + 2 * by) % 8) for i in range(8)])]
    unnamed x96 -> x58, local copies, waits for them, and re-layouts: 20.1 us -> 13.8 us
    ppermute x6, waiting for transfers between devices: 6.16 us -> 0.02 us  [swapped(): return lax.ppermute(block, 'tp', [(i, i ^ 1) for i in range(8)])]
    ppermute x6, starting transfers between devices: 10.9 us -> 5.15 us  [swapped(): return lax.ppermute(block, 'tp', [(i, i ^ 1) for i in range(8)])]
    all_to_all x1, waiting for transfers between devices: 7.46 us -> 1.81 us  [whole_body(): lax.all_to_all(expert_sum, 'tp', split_axis=0, concat_axis=1, tiled=True)]
    all_to_all x1, waiting for transfers between devices: 5.25 us -> 0.01 us  [whole_body(): lax.all_to_all(results.reshape(experts, capacity, -1), 'ep', 0, 0, tiled=...]
    ppermute x1, waiting for transfers between devices: 28.7 us -> 31.7 us  [whole_body(): halo = lax.ppermute(tail, 'ep', [(i, i + 1) for i in range(15)])]
    ppermute x12, waiting for transfers between devices: 19.9 us -> 22.7 us  [turned(): return lax.ppermute(block, 'tp', [(i, (i + 2 * by) % 8) for i in range(8)])]
  transfers between devices with their start and end apart: 23 -> 23, of which waited for: 9 -> 9; matrix products, arithmetic and copies ran while one was open for 5% -> 8% of each run, Pallas kernels for 9% -> 12%
where the time goes in v2:
time: 180 us; the launch traced here: 179 us
  starting transfers between devices  59.9 us (33%)
  waiting for transfers between devices  56.3 us (31%)
  Pallas kernels  33 us (18%)
  local copies, waits for them, and re-layouts  16.8 us (9%)
  other arithmetic  9.94 us (6%)
  matrix products  2.03 us (1%)
    ppermute x1, waiting for transfers between devices, whole_body(): halo = lax.ppermute(tail, 'ep', [(i, i + 1) for i in range(15)])  31.7 us
    ppermute x12, waiting for transfers between devices, turned(): return lax.ppermute(block, 'tp', [(i, (i + 2 * by) % 8) for i in range(8)])  22.7 us
    ppermute x12, starting transfers between devices, turned(): return lax.ppermute(block, 'tp', [(i, (i + 2 * by) % 8) for i in range(8)])  22.4 us
    unnamed x58, local copies, waits for them, and re-layouts  13.8 us
    pallas_call x1, Pallas kernels, mixer_local(): pl.pallas_call(mixer_kernel, out_shape=(full, full, full, jax.ShapeDtypeS...  10.3 us
    all_to_all x1, starting transfers between devices, whole_body(): lax.all_to_all(jnp.broadcast_to(carry[None], (experts, *carry.shape)), 'e...  9.57 us
    all_to_all x1, starting transfers between devices, whole_body(): lax.all_to_all(outgoing.reshape(experts, capacity, half), 'ep', 0, 0, til...  8.6 us
    pallas_call x1, Pallas kernels, expert_front(): pl.pallas_call(functools.partial(front_kernel, experts=experts, capacity=...  7.07 us
  transfers between devices with their start and end apart: 23, of which 9 were waited for; matrix products, arithmetic and copies ran while one was open for 8% of the time, Pallas kernels for 12%

profile of v2, /device:TPU:1, one launch (start us, length us, event | category | flops | bytes accessed | tf_op | source)
XLA Modules:
  0.0 179.0 jit_solution(10078595584505889541)
XLA Ops:
  0.6 0.0 copy-start
  0.6 7.1 %expert_front.1 = (bf16[768,2048]{1,0:T(8,128)(2,1)}, bf16[256,4096]{1,0:T(8,128)(2,1)}, s32[2,256]{1,0:T(2,128)}, bf16[8,4096]{1,0:T(8,128)(2,1)}) custom-call(bf16[256,4096]{1,0:T(8,128)(2,1)} %rows_hbm.1, f32[1,4096]{1,0:T(1,128)} %bitcast.51, s32[2,256]{1,0:T(2,128)} %bitcast.53, bf16[256,4096]{1,0:T(8,128)(2,1)} %rows_hbm.2), custom_call_target="tpu_custom_call" | custom-call | flops 5000000000 | bytes 5000000 | tf_op jit(solution)/shard_map/expert_front/pallas_call | solution.py:227
  7.7 8.6 %all-to-all-start = ((bf16[16,48,2048]{2,1,0:T(8,128)(2,1)}), bf16[16,48,2048]{2,1,0:T(8,128)(2,1)}, u32[]{:S(2)}, u32[]{:S(2)}) async-start(bf16[16,48,2048]{2,1,0:T(8,128)(2,1)} %bitcast.47), calls=%async_computation | async-start | bytes 6291456 | tf_op jit(solution)/shard_map/all_to_all | solution.py:523
  16.4 3.2 %collective-permute-start = (bf16[8,4096]{1,0:T(8,128)(2,1)S(1)}, bf16[8,4096]{1,0:T(8,128)(2,1)S(1)}, u32[]{:S(2)}, u32[]{:S(2)}) collective-permute-start(bf16[8,4096]{1,0:T(8,128)(2,1)S(1)} %copy-done.27), channel_id=1, source_target_pairs={{0,8},{8,16},{16,24},{24,32},{32,40},{40,48},{48,56},{56,64},{64,7... | collective-permute-start | bytes 196616 | tf_op jit(solution)/shard_map/ppermute | solution.py:522
  19.6 3.0 %prepared.1 = (bf16[2048,128]{1,0:T(8,128)(2,1)}, bf16[2048,128]{1,0:T(8,128)(2,1)}, bf16[256,1024]{1,0:T(8,128)(2,1)}, bf16[256,1024]{1,0:T(8,128)(2,1)}, bf16[...) custom-call(bf16[4096,128]{1,0:T(8,128)(2,1)} %bitcast.41, bf16[4096,128]{1,0:T(8,128)(2,1)} %bitcast.43, ...), custom_call_target="tpu_custom_call" | custom-call | flops 3000000000 | bytes 3000000 | tf_op jit(solution)/shard_map/prepared/pallas_call | solution.py:344
  22.6 1.6 collective-permute-start.2
  24.2 0.1 collective-permute-start.1
  24.3 0.7 fusion.8
  25.0 1.3 fusion.refs_0_
  26.4 31.7 %collective-permute-done.halo = bf16[8,4096]{1,0:T(8,128)(2,1)S(1)} collective-permute-done((bf16[8,4096]{1,0:T(8,128)(2,1)S(1)}, bf16[8,4096]{1,0:T(8,128)(2,1)S(1)}, u32[]{:S(2)}, u32[]{:S(2)}) %collective-permute-start) | collective-permute-done | bytes 65568 | tf_op jit(solution)/shard_map/ppermute | solution.py:522
  58.1 0.6 copy-done.28
  58.7 10.3 %mixer_local.1 = (f32[256,512]{1,0:T(8,128)}, f32[256,512]{1,0:T(8,128)}, f32[256,512]{1,0:T(8,128)}, f32[2,512]{1,0:T(2,128)}) custom-call(bf16[256,4096]{1,0:T(8,128)(2,1)} %rows_hbm.2, bf16[8,4096]{1,0:T(8,128)(2,1)} %copy-done.28, f32[1,4096]{1,0:T(1,128)} %bitcast.52, bf16[4096,512]{1,0:T(8,128)(2,1)} %gate_hbm.1, bf16[4096,512]{1,0:T(8,128)(2,1)} %input_hbm.1, ...), custom_call_target="tpu_custom_call" | custom-call | flops 8000000000 | bytes 8000000 | tf_op jit(solution)/shard_map/mixer_local/pallas_call | solution.py:142
  69.1 4.0 %expert_parts.1 = (f32[768,256]{1,0:T(8,128)S(1)}, f32[768,256]{1,0:T(8,128)S(1)}) custom-call(bf16[768,2048]{1,0:T(8,128)(2,1)} %bitcast.8.received_hbm, bf16[4096,128]{1,0:T(8,128)(2,1)S(1)} %bitcast.42, bf16[4096,128]{1,0:T(8,128)(2,1)S(1)} %bitcast.44, bf16[2048,128]{1,0:T(8,128)(2,1)} %collective-permute-done.1.refs_2_, ...), custom_call_target="tpu_custom_call" | custom-call | flops 5000000000 | bytes 5000000 | tf_op jit(solution)/shard_map/expert_parts/pallas_call | solution.py:287
  73.1 1.6 collective-permute-start.3
  74.8 1.3 collective-permute-start.7
  76.1 1.4 collective-permute-start.8
  77.5 1.6 collective-permute-start.9
  79.2 0.1 add.76
  79.3 0.1 fusion.4.refs_0_
  79.4 1.4 collective-permute-start.6
  80.8 1.5 collective-permute-start.5
  82.2 7.2 %collective-permute-done.7.refs_5_ = bf16[256,1024]{1,0:T(8,128)(2,1)S(1)} collective-permute-done((bf16[256,1024]{1,0:T(8,128)(2,1)S(1)}, bf16[256,1024]{1,0:T(8,128)(2,1)S(1)}, u32[]{:S(2)}, u32[]{:S(2)}) %collective-permute-start.7) | collective-permute-done | bytes 524320 | tf_op jit(solution)/shard_map/ppermute | solution.py:495
  89.5 0.6 broadcast_in_dim.2
  90.1 9.6 %all-to-all-start.1 = ((f32[16,2,512]{2,1,0:T(2,128)}), f32[16,2,512]{2,1,0:T(2,128)}, u32[]{:S(2)}, u32[]{:S(2)}) async-start(f32[16,2,512]{2,1,0:T(2,128)} %broadcast_in_dim.2), calls=%async_computation.1 | async-start | bytes 131072 | tf_op jit(solution)/shard_map/all_to_all | solution.py:551
  99.7 0.8 copy-done.4
  100.5 1.4 collective-permute-done.9.refs_7_
  101.9 0.8 copy-done.7
  102.7 3.4 %collective-permute-done.6.refs_3_ = bf16[768,128]{1,0:T(8,128)(2,1)S(1)} collective-permute-done((bf16[768,128]{1,0:T(8,128)(2,1)S(1)}, bf16[768,128]{1,0:T(8,128)(2,1)S(1)}, u32[]{:S(2)}, u32[]{:S(2)}) %collective-permute-start.6) | collective-permute-done | bytes 196640 | tf_op jit(solution)/shard_map/ppermute | solution.py:495
  106.1 3.0 %collective-permute-done.5.refs_2_ = bf16[768,128]{1,0:T(8,128)(2,1)S(1)} collective-permute-done((bf16[768,128]{1,0:T(8,128)(2,1)S(1)}, bf16[768,128]{1,0:T(8,128)(2,1)S(1)}, u32[]{:S(2)}, u32[]{:S(2)}) %collective-permute-start.5) | collective-permute-done | bytes 196640 | tf_op jit(solution)/shard_map/ppermute | solution.py:495
  109.1 0.7 copy-done.10
  109.8 0.9 collective-permute-done.4.refs_1_
  110.7 0.7 copy-done.12
  111.4 1.0 copy-done.5
  112.4 1.0 copy-done.8
  113.5 0.9 copy-done.11
  114.4 0.9 copy-done.13
  115.3 1.0 copy-done.16
  116.4 1.1 down_parts.2
  117.6 1.2 copy-done.1
  118.8 0.5 collective-permute-start.14
  119.3 5.5 %mixer_out.1 = (f32[128,4096]{1,0:T(8,128)}, f32[128,4096]{1,0:T(8,128)}) custom-call(f32[256,512]{1,0:T(8,128)} %get-tuple-element.36.gate_hbm, f32[256,512]{1,0:T(8,128)} %get-tuple-element.37.states_hbm, f32[256,512]{1,0:T(8,128)} %get-tuple-element.38.decays_hbm, f32[16,2,512]{2,1,0:T(2,128)} %all-to-all-done.1.carries, bf16[512,4096]{1,0:T(8,128)(2,1)} %out_hbm.1), custom_call_target="tpu_custom_call" | custom-call | flops 3000000000 | bytes 3000000 | tf_op jit(solution)/shard_map/mixer_out/pallas_call | solution.py:440
  124.7 0.1 collective-permute-start.10
  124.8 8.7 %collective-permute-start.17 = (bf16[256,128]{1,0:T(8,128)(2,1)S(1)}, bf16[256,128]{1,0:T(8,128)(2,1)S(1)}, u32[]{:S(2)}, u32[]{:S(2)}) collective-permute-start(bf16[256,128]{1,0:T(8,128)(2,1)S(1)} %copy-done.14), channel_id=1, source_target_pairs={{0,4},{1,5},{2,6},{3,7},{4,0},{5,1},{6,2},{7,3},{8,12},{9,13},{10,... | collective-permute-start | bytes 196616 | tf_op jit(solution)/shard_map/ppermute | solution.py:495
  133.5 2.3 %collective-permute-start.16 = (bf16[256,128]{1,0:T(8,128)(2,1)S(1)}, bf16[256,128]{1,0:T(8,128)(2,1)S(1)}, u32[]{:S(2)}, u32[]{:S(2)}) collective-permute-start(bf16[256,128]{1,0:T(8,128)(2,1)S(1)} %copy-done.14), channel_id=1, source_target_pairs={{0,6},{1,7},{2,0},{3,1},{4,2},{5,3},{6,4},{7,5},{8,14},{9,15},{10,... | collective-permute-start | bytes 196616 | tf_op jit(solution)/shard_map/ppermute | solution.py:495
  135.9 1.2 add_convert_fusion
  137.0 6.9 %all-to-all-start.2 = ((bf16[16,48,512]{2,1,0:T(8,128)(2,1)}), bf16[16,48,512]{2,1,0:T(8,128)(2,1)S(1)}, u32[]{:S(2)}, u32[]{:S(2)}) async-start(bf16[16,48,512]{2,1,0:T(8,128)(2,1)} %bitcast.48), calls=%async_computation.2 | async-start | bytes 1572864 | tf_op jit(solution)/shard_map/all_to_all | solution.py:560
  144.0 1.0 copy-done.6
  145.0 1.0 copy-done.9
  146.0 1.0 copy-done.17
  147.1 0.6 down_parts.3
  147.7 0.8 copy-done.18
  148.5 1.2 collective-permute-start.18
  149.8 3.9 %add.78 = f32[128,4096]{1,0:T(8,128)} add(f32[128,4096]{1,0:T(8,128)} %get-tuple-element.52, f32[128,4096]{1,0:T(8,128)} %collective-permute-done.10) | non-fusion elementwise | flops 524288 | bytes 6291456 | tf_op jit(solution)/shard_map/add | solution.py:568
  153.7 2.3 %fusion.5 = (bf16[32,4096]{1,0:T(8,128)(2,1)}, bf16[32,4096]{1,0:T(8,128)(2,1)}, bf16[32,4096]{1,0:T(8,128)(2,1)}) fusion(f32[4,32,4096]{2,1,0:T(8,128)} %bitcast.9, s32[]{:T(128)S(6)} %select_n.35, s32[]{:T(128)S(6)} %select_n.39, s32[]{:T(128)S(6)} %select_n.37), kind=kLoop, calls=%fused_computation.16 | loop fusion | bytes 1572876 | tf_op jit(solution)/shard_map/convert_element_type | solution.py:572
  155.9 4.1 %collective-permute-start.13 = (bf16[32,4096]{1,0:T(8,128)(2,1)}, bf16[32,4096]{1,0:T(8,128)(2,1)}, u32[]{:S(2)}, u32[]{:S(2)}) collective-permute-start(bf16[32,4096]{1,0:T(8,128)(2,1)} %get-tuple-element.59), channel_id=1, source_target_pairs={{0,4},{1,5},{2,6},{3,7},{4,0},{5,1},{6,2},{7,3},{8,12},{9,13},{10,... | collective-permute-start | bytes 786440 | tf_op jit(solution)/shard_map/ppermute | solution.py:495
  160.1 1.4 combine.1
  161.6 4.1 %all-to-all-start.3 = ((f32[8,32,512]{2,1,0:T(8,128)}), f32[8,32,512]{2,1,0:T(8,128)S(1)}, u32[]{:S(2)}, u32[]{:S(2)}) async-start(f32[8,32,512]{2,1,0:T(8,128)} %bitcast.17), calls=%async_computation.3 | async-start | bytes 1048576 | tf_op jit(solution)/shard_map/all_to_all | solution.py:577
  165.7 0.2 collective-permute-done.11
  165.9 6.6 %collective-permute-done.13 = bf16[32,4096]{1,0:T(8,128)(2,1)} collective-permute-done((bf16[32,4096]{1,0:T(8,128)(2,1)}, bf16[32,4096]{1,0:T(8,128)(2,1)}, u32[]{:S(2)}, u32[]{:S(2)}) %collective-permute-start.13) | collective-permute-done | bytes 262176 | tf_op jit(solution)/shard_map/ppermute | solution.py:495
  172.4 1.5 multiply_reduce_fusion
  174.0 2.1 %multiply_convert_fusion.1 = bf16[32,4096]{1,0:T(8,128)(2,1)} fusion(f32[4096]{0:T(1024)S(1)} %copy-done.22, f32[32]{0:T(128)S(1)} %add_rsqrt_fusion.1, bf16[32,4096]{1,0:T(8,128)(2,1)} %collective-permute-done.13, bf16[32,4096]{1,0:T(8,128)(2,1)} %collective-permute-done.12, bf16[32,4096]{1,0:T(8,128)(2,1)} %collective-permute-done.11, ...), kind=kLoop, calls=%fused_computation.9 | loop fusion | flops 1179648 | bytes 1589380 | tf_op jit(solution)/shard_map/convert_element_type | solution.py:574
  176.1 1.8 %all-to-all-done.3 = f32[8,32,512]{2,1,0:T(8,128)S(1)} async-done(((f32[8,32,512]{2,1,0:T(8,128)}), f32[8,32,512]{2,1,0:T(8,128)S(1)}, u32[]{:S(2)}, u32[]{:S(2)}) %all-to-all-start.3) | async-done | bytes 524320 | tf_op jit(solution)/shard_map/all_to_all | solution.py:577
  177.9 0.2 fusion.1
  178.2 0.8 multiply_convert_fusion
  (63 shorter events, 0.2 us)
Async XLA Ops:
  0.6 23.7 %copy-start = (bf16[4096,128]{1,0:T(8,128)(2,1)S(1)}, bf16[4096,128]{1,0:T(8,128)(2,1)}, u32[]{:S(2)}) copy-start(bf16[4096,128]{1,0:T(8,128)(2,1)} %param.38) | copy-start | bytes 3145732
  7.7 8.6 %copy-start.27 = (bf16[8,4096]{1,0:T(8,128)(2,1)S(1)}, bf16[8,4096]{1,0:T(8,128)(2,1)}, u32[]{:S(2)}) copy-start(bf16[8,4096]{1,0:T(8,128)(2,1)} %get-tuple-element.35) | copy-start | bytes 196612
  7.7 61.3 %all-to-all-start = ((bf16[16,48,2048]{2,1,0:T(8,128)(2,1)}), bf16[16,48,2048]{2,1,0:T(8,128)(2,1)}, u32[]{:S(2)}, u32[]{:S(2)}) async-start(bf16[16,48,2048]{2,1,0:T(8,128)(2,1)} %bitcast.47), calls=%async_computation | async-start | bytes 6291456 | tf_op jit(solution)/shard_map/all_to_all | solution.py:523
  16.4 41.7 %collective-permute-start = (bf16[8,4096]{1,0:T(8,128)(2,1)S(1)}, bf16[8,4096]{1,0:T(8,128)(2,1)S(1)}, u32[]{:S(2)}, u32[]{:S(2)}) collective-permute-start(bf16[8,4096]{1,0:T(8,128)(2,1)S(1)} %copy-done.27), channel_id=1, source_target_pairs={{0,8},{8,16},{16,24},{24,32},{32,40},{40,48},{48,56},{56,64},{64,7... | collective-permute-start | bytes 196616 | tf_op jit(solution)/shard_map/ppermute | solution.py:522
  19.6 4.7 %copy-start.21 = (bf16[256,4096]{1,0:T(8,128)(2,1)S(1)}, bf16[256,4096]{1,0:T(8,128)(2,1)}, u32[]{:S(2)}) copy-start(bf16[256,4096]{1,0:T(8,128)(2,1)} %get-tuple-element.30) | copy-start | bytes 6291460
  22.6 2.4 %copy-start.25 = (bf16[4096,128]{1,0:T(8,128)(2,1)S(1)}, bf16[4096,128]{1,0:T(8,128)(2,1)}, u32[]{:S(2)}) copy-start(bf16[4096,128]{1,0:T(8,128)(2,1)} %param.39) | copy-start | bytes 3145732
  22.6 46.4 %collective-permute-start.2 = (bf16[2048,128]{1,0:T(8,128)(2,1)}, bf16[2048,128]{1,0:T(8,128)(2,1)}, u32[]{:S(2)}, u32[]{:S(2)}) collective-permute-start(bf16[2048,128]{1,0:T(8,128)(2,1)} %get-tuple-element.42), channel_id=1, source_target_pairs={{0,1},{1,0},{2,3},{3,2},{4,5},{5,4},{6,7},{7,6},{8,9},{9,8},{10,11... | collective-permute-start | bytes 1572872 | tf_op jit(solution)/shard_map/ppermute | solution.py:491
  24.2 44.9 %collective-permute-start.1 = (bf16[2048,128]{1,0:T(8,128)(2,1)}, bf16[2048,128]{1,0:T(8,128)(2,1)}, u32[]{:S(2)}, u32[]{:S(2)}) collective-permute-start(bf16[2048,128]{1,0:T(8,128)(2,1)} %get-tuple-element.33), channel_id=1, source_target_pairs={{0,1},{1,0},{2,3},{3,2},{4,5},{5,4},{6,7},{7,6},{8,9},{9,8},{10,11... | collective-permute-start | bytes 1572872 | tf_op jit(solution)/shard_map/ppermute | solution.py:491
  58.1 0.6 copy-start.28
  58.7 10.3 %copy-start.2 = (bf16[1,4096,128]{2,1,0:T(8,128)(2,1)S(1)}, bf16[1,4096,128]{2,1,0:T(8,128)(2,1)}, u32[]{:S(2)}) copy-start(bf16[1,4096,128]{2,1,0:T(8,128)(2,1)} %param.35) | copy-start | bytes 3145732
  58.7 10.3 %copy-start.3 = (bf16[1,4096,128]{2,1,0:T(8,128)(2,1)S(1)}, bf16[1,4096,128]{2,1,0:T(8,128)(2,1)}, u32[]{:S(2)}) copy-start(bf16[1,4096,128]{2,1,0:T(8,128)(2,1)} %param.36) | copy-start | bytes 3145732
  69.0 5.7 %copy-start.26 = (bf16[256,1024]{1,0:T(8,128)(2,1)S(1)}, bf16[256,1024]{1,0:T(8,128)(2,1)}, u32[]{:S(2)}) copy-start(bf16[256,1024]{1,0:T(8,128)(2,1)} %get-tuple-element.47) | copy-start | bytes 1572868
  73.1 16.4 %copy-start.24 = (f32[2,512]{1,0:T(2,128)S(1)}, f32[2,512]{1,0:T(2,128)}, u32[]{:S(2)}) copy-start(f32[2,512]{1,0:T(2,128)} %get-tuple-element.45) | copy-start | bytes 12292
  73.1 6.0 %collective-permute-start.3 = (f32[768,256]{1,0:T(8,128)S(1)}, f32[768,256]{1,0:T(8,128)S(1)}, u32[]{:S(2)}, u32[]{:S(2)}) collective-permute-start(f32[768,256]{1,0:T(8,128)S(1)} %get-tuple-element.44), channel_id=1, source_target_pairs={{0,1},{1,0},{2,3},{3,2},{4,5},{5,4},{6,7},{7,6},{8,9},{9,8},{10,11... | collective-permute-start | bytes 2359304 | tf_op jit(solution)/shard_map/ppermute | solution.py:491
  74.8 14.7 %collective-permute-start.7 = (bf16[256,1024]{1,0:T(8,128)(2,1)S(1)}, bf16[256,1024]{1,0:T(8,128)(2,1)S(1)}, u32[]{:S(2)}, u32[]{:S(2)}) collective-permute-start(bf16[256,1024]{1,0:T(8,128)(2,1)S(1)} %copy-done.26), channel_id=1, source_target_pairs={{0,2},{1,3},{2,4},{3,5},{4,6},{5,7},{6,0},{7,1},{8,10},{9,11},{10,... | collective-permute-start | bytes 1572872 | tf_op jit(solution)/shard_map/ppermute | solution.py:495
  76.1 23.6 %collective-permute-start.8 = (bf16[256,1024]{1,0:T(8,128)(2,1)}, bf16[256,1024]{1,0:T(8,128)(2,1)S(1)}, u32[]{:S(2)}, u32[]{:S(2)}) collective-permute-start(bf16[256,1024]{1,0:T(8,128)(2,1)} %get-tuple-element.48), channel_id=1, source_target_pairs={{0,6},{1,7},{2,0},{3,1},{4,2},{5,3},{6,4},{7,5},{8,14},{9,15},{10,... | collective-permute-start | bytes 1572872 | tf_op jit(solution)/shard_map/ppermute | solution.py:495
  77.5 24.4 %collective-permute-start.9 = (bf16[256,1024]{1,0:T(8,128)(2,1)}, bf16[256,1024]{1,0:T(8,128)(2,1)S(1)}, u32[]{:S(2)}, u32[]{:S(2)}) collective-permute-start(bf16[256,1024]{1,0:T(8,128)(2,1)} %get-tuple-element.49), channel_id=1, source_target_pairs={{0,4},{1,5},{2,6},{3,7},{4,0},{5,1},{6,2},{7,3},{8,12},{9,13},{10,... | collective-permute-start | bytes 1572872 | tf_op jit(solution)/shard_map/ppermute | solution.py:495
  79.4 26.7 %collective-permute-start.6 = (bf16[768,128]{1,0:T(8,128)(2,1)S(1)}, bf16[768,128]{1,0:T(8,128)(2,1)S(1)}, u32[]{:S(2)}, u32[]{:S(2)}) collective-permute-start(bf16[768,128]{1,0:T(8,128)(2,1)S(1)} %fusion.4.refs_0_), channel_id=1, source_target_pairs={{0,4},{1,5},{2,6},{3,7},{4,0},{5,1},{6,2},{7,3},{8,12},{9,13},{10,... | collective-permute-start | bytes 589832 | tf_op jit(solution)/shard_map/ppermute | solution.py:495
  80.8 28.3 %collective-permute-start.5 = (bf16[768,128]{1,0:T(8,128)(2,1)S(1)}, bf16[768,128]{1,0:T(8,128)(2,1)S(1)}, u32[]{:S(2)}, u32[]{:S(2)}) collective-permute-start(bf16[768,128]{1,0:T(8,128)(2,1)S(1)} %fusion.4.refs_0_), channel_id=1, source_target_pairs={{0,6},{1,7},{2,0},{3,1},{4,2},{5,3},{6,4},{7,5},{8,14},{9,15},{10,... | collective-permute-start | bytes 589832 | tf_op jit(solution)/shard_map/ppermute | solution.py:495
  89.5 21.2 %collective-permute-start.4 = (bf16[768,128]{1,0:T(8,128)(2,1)S(1)}, bf16[768,128]{1,0:T(8,128)(2,1)S(1)}, u32[]{:S(2)}, u32[]{:S(2)}) collective-permute-start(bf16[768,128]{1,0:T(8,128)(2,1)S(1)} %fusion.4.refs_0_), channel_id=1, source_target_pairs={{0,2},{1,3},{2,4},{3,5},{4,6},{5,7},{6,0},{7,1},{8,10},{9,11},{10,... | collective-permute-start | bytes 589832 | tf_op jit(solution)/shard_map/ppermute | solution.py:495
  90.1 28.7 %all-to-all-start.1 = ((f32[16,2,512]{2,1,0:T(2,128)}), f32[16,2,512]{2,1,0:T(2,128)}, u32[]{:S(2)}, u32[]{:S(2)}) async-start(f32[16,2,512]{2,1,0:T(2,128)} %broadcast_in_dim.2), calls=%async_computation.1 | async-start | bytes 131072 | tf_op jit(solution)/shard_map/all_to_all | solution.py:551
  99.7 0.8 copy-start.4
  101.9 0.8 copy-start.7
  109.1 0.7 copy-start.10
  110.7 0.7 copy-start.12
  111.4 1.0 copy-start.5
  112.4 1.0 copy-start.8
  113.5 0.9 copy-start.11
  114.4 0.9 copy-start.13
  115.3 1.0 copy-start.16
  117.5 1.2 copy-start.1
  118.8 17.1 %collective-permute-start.14 = (f32[768,512]{1,0:T(8,128)}, f32[768,512]{1,0:T(8,128)S(1)}, u32[]{:S(2)}, u32[]{:S(2)}) collective-permute-start(f32[768,512]{1,0:T(8,128)} %copy-done.1), channel_id=1, source_target_pairs={{0,1},{1,0},{2,3},{3,2},{4,5},{5,4},{6,7},{7,6},{8,9},{9,8},{10,11... | collective-permute-start | bytes 4718600 | tf_op jit(solution)/shard_map/ppermute | solution.py:491
  119.3 5.6 %copy-start.14 = (bf16[256,128]{1,0:T(8,128)(2,1)S(1)}, bf16[256,128]{1,0:T(8,128)(2,1)}, u32[]{:S(2)}) copy-start(bf16[256,128]{1,0:T(8,128)(2,1)} %fusion.refs_0_) | copy-start | bytes 196612
  124.7 25.0 %collective-permute-start.10 = (f32[128,4096]{1,0:T(8,128)}, f32[128,4096]{1,0:T(8,128)}, u32[]{:S(2)}, u32[]{:S(2)}) collective-permute-start(f32[128,4096]{1,0:T(8,128)} %get-tuple-element.53), channel_id=1, source_target_pairs={{0,1},{1,0},{2,3},{3,2},{4,5},{5,4},{6,7},{7,6},{8,9},{9,8},{10,11... | collective-permute-start | bytes 6291464 | tf_op jit(solution)/shard_map/ppermute | solution.py:491
  124.8 19.1 %collective-permute-start.17 = (bf16[256,128]{1,0:T(8,128)(2,1)S(1)}, bf16[256,128]{1,0:T(8,128)(2,1)S(1)}, u32[]{:S(2)}, u32[]{:S(2)}) collective-permute-start(bf16[256,128]{1,0:T(8,128)(2,1)S(1)} %copy-done.14), channel_id=1, source_target_pairs={{0,4},{1,5},{2,6},{3,7},{4,0},{5,1},{6,2},{7,3},{8,12},{9,13},{10,... | collective-permute-start | bytes 196616 | tf_op jit(solution)/shard_map/ppermute | solution.py:495
  133.5 10.4 %collective-permute-start.16 = (bf16[256,128]{1,0:T(8,128)(2,1)S(1)}, bf16[256,128]{1,0:T(8,128)(2,1)S(1)}, u32[]{:S(2)}, u32[]{:S(2)}) collective-permute-start(bf16[256,128]{1,0:T(8,128)(2,1)S(1)} %copy-done.14), channel_id=1, source_target_pairs={{0,6},{1,7},{2,0},{3,1},{4,2},{5,3},{6,4},{7,5},{8,14},{9,15},{10,... | collective-permute-start | bytes 196616 | tf_op jit(solution)/shard_map/ppermute | solution.py:495
  135.9 8.1 %collective-permute-start.15 = (bf16[256,128]{1,0:T(8,128)(2,1)S(1)}, bf16[256,128]{1,0:T(8,128)(2,1)S(1)}, u32[]{:S(2)}, u32[]{:S(2)}) collective-permute-start(bf16[256,128]{1,0:T(8,128)(2,1)S(1)} %copy-done.14), channel_id=1, source_target_pairs={{0,2},{1,3},{2,4},{3,5},{4,6},{5,7},{6,0},{7,1},{8,10},{9,11},{10,... | collective-permute-start | bytes 196616 | tf_op jit(solution)/shard_map/ppermute | solution.py:495
  137.0 23.1 %all-to-all-start.2 = ((bf16[16,48,512]{2,1,0:T(8,128)(2,1)}), bf16[16,48,512]{2,1,0:T(8,128)(2,1)S(1)}, u32[]{:S(2)}, u32[]{:S(2)}) async-start(bf16[16,48,512]{2,1,0:T(8,128)(2,1)} %bitcast.48), calls=%async_computation.2 | async-start | bytes 1572864 | tf_op jit(solution)/shard_map/all_to_all | solution.py:560
  143.9 1.0 copy-start.6
  145.0 1.0 copy-start.9
  146.0 1.0 copy-start.17
  147.7 0.9 copy-start.18
  148.5 11.6 %collective-permute-start.18 = (f32[256,512]{1,0:T(8,128)S(1)}, f32[256,512]{1,0:T(8,128)S(1)}, u32[]{:S(2)}, u32[]{:S(2)}) collective-permute-start(f32[256,512]{1,0:T(8,128)S(1)} %get-tuple-element.57), channel_id=1, source_target_pairs={{0,1},{1,0},{2,3},{3,2},{4,5},{5,4},{6,7},{7,6},{8,9},{9,8},{10,11... | collective-permute-start | bytes 1572872 | tf_op jit(solution)/shard_map/ppermute | solution.py:491
  149.8 10.3 %copy-start.15 = (f32[256,2]{0,1:T(2,128)S(1)}, f32[256,2]{0,1:T(2,128)}, u32[]{:S(2)}) copy-start(f32[256,2]{0,1:T(2,128)} %param.34) | copy-start | bytes 6148
  149.8 10.3 %copy-start.19 = (f32[256,512]{1,0:T(8,128)S(1)}, f32[256,512]{1,0:T(8,128)}, u32[]{:S(2)}) copy-start(f32[256,512]{1,0:T(8,128)} %copy-done.18) | copy-start | bytes 1572868
  149.8 10.3 %copy-start.20 = (s32[2,256]{1,0:T(2,128)S(1)}, s32[2,256]{1,0:T(2,128)}, u32[]{:S(2)}) copy-start(s32[2,256]{1,0:T(2,128)} %get-tuple-element.31.slots) | copy-start | bytes 6148
  155.9 9.9 %collective-permute-start.11 = (bf16[32,4096]{1,0:T(8,128)(2,1)}, bf16[32,4096]{1,0:T(8,128)(2,1)}, u32[]{:S(2)}, u32[]{:S(2)}) collective-permute-start(bf16[32,4096]{1,0:T(8,128)(2,1)} %get-tuple-element.58), channel_id=1, source_target_pairs={{0,2},{1,3},{2,4},{3,5},{4,6},{5,7},{6,0},{7,1},{8,10},{9,11},{10,... | collective-permute-start | bytes 786440 | tf_op jit(solution)/shard_map/ppermute | solution.py:495
  155.9 16.5 %collective-permute-start.13 = (bf16[32,4096]{1,0:T(8,128)(2,1)}, bf16[32,4096]{1,0:T(8,128)(2,1)}, u32[]{:S(2)}, u32[]{:S(2)}) collective-permute-start(bf16[32,4096]{1,0:T(8,128)(2,1)} %get-tuple-element.59), channel_id=1, source_target_pairs={{0,4},{1,5},{2,6},{3,7},{4,0},{5,1},{6,2},{7,3},{8,12},{9,13},{10,... | collective-permute-start | bytes 786440 | tf_op jit(solution)/shard_map/ppermute | solution.py:495
  160.1 12.4 %collective-permute-start.12 = (bf16[32,4096]{1,0:T(8,128)(2,1)}, bf16[32,4096]{1,0:T(8,128)(2,1)}, u32[]{:S(2)}, u32[]{:S(2)}) collective-permute-start(bf16[32,4096]{1,0:T(8,128)(2,1)} %get-tuple-element.60), channel_id=1, source_target_pairs={{0,6},{1,7},{2,0},{3,1},{4,2},{5,3},{6,4},{7,5},{8,14},{9,15},{10,... | collective-permute-start | bytes 786440 | tf_op jit(solution)/shard_map/ppermute | solution.py:495
  161.6 12.4 %copy-start.22 = (f32[4096]{0:T(1024)S(1)}, f32[4096]{0:T(1024)}, u32[]{:S(2)}) copy-start(f32[4096]{0:T(1024)} %param.30) | copy-start | bytes 49156
  161.6 16.4 %all-to-all-start.3 = ((f32[8,32,512]{2,1,0:T(8,128)}), f32[8,32,512]{2,1,0:T(8,128)S(1)}, u32[]{:S(2)}, u32[]{:S(2)}) async-start(f32[8,32,512]{2,1,0:T(8,128)} %bitcast.17), calls=%async_computation.3 | async-start | bytes 1048576 | tf_op jit(solution)/shard_map/all_to_all | solution.py:577
  165.7 12.5 %copy-start.23 = (f32[4096]{0:T(1024)S(1)}, f32[4096]{0:T(1024)}, u32[]{:S(2)}) copy-start(f32[4096]{0:T(1024)} %param.41) | copy-start | bytes 49156
